TPU v7x, 256 devices: a whole 4x4x8 slice. The times are simulated.
256 devices in a mesh: sp: 64 (over z, y, core), tp: 4 (over x).
Axes of the slice: x: 4, y: 4, z: 8, core: 2. Of those that a mesh axis runs over, the one named last changes fastest.
Arguments:
- resid: bfloat16 [24576, 2048], P(('sp', 'tp')), may hold values from -6 to 6
- conv_b: bfloat16 [24576, 1024], P('sp', 'tp'), may hold values from -6 to 6
- conv_c: bfloat16 [24576, 1024], P('sp', 'tp'), may hold values from -6 to 6
- conv_x: bfloat16 [24576, 1024], P('sp', 'tp'), may hold values from -6 to 6
- conv_taps: bfloat16 [3, 1024], P(None, 'tp'), may hold values from -3.5 to 3.5
- out_weight: bfloat16 [1024, 2048], P('tp'), may hold values from -0.1875 to 0.1875
- norm_gain: float32 [2048], replicated, may hold values from 0.1 to 1.9
- routes: int32 [24576, 2], P('sp'), may hold values from 0 to 63, all different within a row; in each aligned block of 96 rows (0 to 95, 96 to 191, ...) at most 4 rows name the same one
- route_weight: float32 [24576, 2], P('sp'), may hold values from 0.2 to 1
- expert_gate: bfloat16 [64, 2048, 1024], P('sp', None, 'tp'), may hold values from -0.125 to 0.125
- expert_up: bfloat16 [64, 2048, 1024], P('sp', None, 'tp'), may hold values from -0.125 to 0.125
- expert_down: bfloat16 [64, 1024, 2048], P('sp', 'tp'), may hold values from -0.1875 to 0.1875
- shared_gate: bfloat16 [2048, 1024], P(None, 'tp'), may hold values from -0.125 to 0.125
- shared_up: bfloat16 [2048, 1024], P(None, 'tp'), may hold values from -0.125 to 0.125
- shared_down: bfloat16 [1024, 2048], P('tp'), may hold values from -0.1875 to 0.1875
Outputs:
- layer_out: bfloat16 [24576, 2048], P(('sp', 'tp'))
Inputs may be any that keep to these rules, and one draw needn't show every extreme that they name: `routes`: in each aligned block of 96 tokens no expert is named more than 4 times; in some blocks some expert is named exactly 4 times; each row names 2 different experts.
All inputs are finite; a program needn't handle non-finite values.
Results may differ from a plain program's by a relative error of at most 0.015.
Values may be sent and summed in bfloat16 or wider, within the bound.
A program may use at most 128 MiB of HBM per device.

v0:
```python
import jax
import jax.numpy as jnp
from jax import lax
from jax.sharding import PartitionSpec as P


def shifted(block, axis, distance):
    devices = range(lax.axis_size(axis))
    route = [(i - distance, i) for i in devices if i - distance in devices]
    return lax.ppermute(block, axis, route)


def round_trip(values):
    return lax.optimization_barrier(values.astype(jnp.bfloat16)).astype(jnp.float32)


def rank_slots(route_rows, expert_count, tp_parts):
    flat_routes = route_rows.reshape(tp_parts, -1)
    onehot = (
        flat_routes[:, :, None] == jnp.arange(expert_count, dtype=jnp.int32)[None, None, :]
    ).astype(jnp.int32)
    slot_ranks = jnp.sum((jnp.cumsum(onehot, axis=1) - 1) * onehot, axis=2)
    return (flat_routes, slot_ranks)


def local(
    resid,
    conv_b,
    conv_c,
    conv_x,
    conv_taps,
    out_weight,
    norm_gain,
    routes,
    route_weight,
    expert_gate,
    expert_up,
    expert_down,
    shared_gate,
    shared_up,
    shared_down,
):
    tok_dev = conv_b.shape[0]
    tp_parts = lax.axis_size("tp")
    groups = lax.axis_size("sp")
    quarter = tok_dev // tp_parts
    tap_count = conv_taps.shape[0]
    exp_dev = expert_gate.shape[0]
    expert_count = exp_dev * groups
    model_width = resid.shape[1]
    top_count = routes.shape[1]
    capacity = max(2, 3 * quarter * top_count // (2 * expert_count))
    my_part = lax.axis_index("tp")
    product = conv_c.astype(jnp.float32) * conv_x.astype(jnp.float32)
    rim_rows = shifted(product[tok_dev - (tap_count - 1) :], "sp", 1)
    padded = jnp.concatenate([rim_rows, product], 0)
    conv_sum = padded[0:tok_dev] * conv_taps[0].astype(jnp.float32)
    for tap_index in range(1, tap_count):
        conv_sum = conv_sum + padded[tap_index : tap_index + tok_dev] * conv_taps[tap_index].astype(
            jnp.float32
        )
    mixed_rows = (conv_b.astype(jnp.float32) * conv_sum).astype(jnp.bfloat16)
    projected = lax.psum_scatter(
        round_trip(jnp.dot(mixed_rows, out_weight, preferred_element_type=jnp.float32)).astype(
            jnp.bfloat16
        ),
        "tp",
        scatter_dimension=0,
        tiled=True,
    ).astype(jnp.float32)
    middle = (resid.astype(jnp.float32) + projected).astype(jnp.bfloat16)
    middle_float = middle.astype(jnp.float32)
    inv_scale = lax.rsqrt(jnp.mean(middle_float * middle_float, axis=-1, keepdims=True) + 1e-06)
    normed = (middle_float * inv_scale * norm_gain).astype(jnp.bfloat16)
    flat_routes, slot_ranks = rank_slots(routes, expert_count, tp_parts)
    own_routes = lax.dynamic_index_in_dim(flat_routes, my_part, 0, keepdims=False)
    own_ranks = lax.dynamic_index_in_dim(slot_ranks, my_part, 0, keepdims=False)
    slot_ids = own_routes * capacity + own_ranks
    token_ids = jnp.repeat(jnp.arange(quarter, dtype=jnp.int32), top_count)
    slot_token = (
        jnp.full((expert_count * capacity,), quarter, jnp.int32).at[slot_ids].set(token_ids)
    )
    padded_rows = jnp.concatenate([normed, jnp.zeros((1, model_width), jnp.bfloat16)], 0)
    outgoing = padded_rows[slot_token].reshape(groups, exp_dev * capacity, model_width)
    arrived = lax.all_to_all(outgoing, "sp", split_axis=0, concat_axis=0, tiled=True)
    arrived = arrived.reshape(groups, exp_dev, capacity, model_width)
    arrived, group_normed = (
        lax.all_gather(arrived, "tp", axis=2, tiled=True),
        lax.all_gather(normed, "tp", axis=0, tiled=True),
    )
    gate_val = jnp.einsum(
        "gerd,edf->gerf", arrived, expert_gate, preferred_element_type=jnp.float32
    )
    up_val = jnp.einsum("gerd,edf->gerf", arrived, expert_up, preferred_element_type=jnp.float32)
    hidden = (jax.nn.silu(gate_val) * up_val).astype(jnp.bfloat16)
    partial_rows = round_trip(
        jnp.einsum("gerf,efd->gerd", hidden, expert_down, preferred_element_type=jnp.float32)
    )
    shared_gate_val = jnp.dot(group_normed, shared_gate, preferred_element_type=jnp.float32)
    shared_up_val = jnp.dot(group_normed, shared_up, preferred_element_type=jnp.float32)
    shared_hidden = (jax.nn.silu(shared_gate_val) * shared_up_val).astype(jnp.bfloat16)
    shared_part = round_trip(
        jnp.dot(shared_hidden, shared_down, preferred_element_type=jnp.float32)
    )
    summed, shared = (
        lax.psum_scatter(
            partial_rows.astype(jnp.bfloat16), "tp", scatter_dimension=2, tiled=True
        ).astype(jnp.float32),
        lax.psum_scatter(
            shared_part.astype(jnp.bfloat16), "tp", scatter_dimension=0, tiled=True
        ).astype(jnp.float32),
    )
    returned = lax.all_to_all(
        summed.astype(jnp.bfloat16), "sp", split_axis=0, concat_axis=0, tiled=True
    )
    returned = returned.reshape(expert_count * capacity, model_width)
    picked = returned[own_routes * capacity + own_ranks].reshape(quarter, top_count, model_width)
    own_weights = lax.dynamic_slice_in_dim(route_weight, my_part * quarter, quarter, 0)
    routed = jnp.sum(picked.astype(jnp.float32) * own_weights[:, :, None], axis=1)
    return (middle.astype(jnp.float32) + shared + routed).astype(jnp.bfloat16)


def solution(mesh):
    return jax.shard_map(
        local,
        mesh=mesh,
        in_specs=(
            P(("sp", "tp"), None),
            P("sp", "tp"),
            P("sp", "tp"),
            P("sp", "tp"),
            P(None, "tp"),
            P("tp", None),
            P(),
            P("sp", None),
            P("sp", None),
            P("sp", None, "tp"),
            P("sp", None, "tp"),
            P("sp", "tp", None),
            P(None, "tp"),
            P(None, "tp"),
            P("tp", None),
        ),
        out_specs=P(("sp", "tp"), None),
        check_vma=False,
    )
```

profile of v0, /device:TPU:1, one launch (start us, length us, event | category | flops | bytes accessed | tf_op | source)
XLA Modules:
  0.0 281.4 jit_solution(15139405090504358709)
XLA Ops:
  6.5 1.1 convert_multiply_fusion.2
  7.7 4.6 %collective-permute-start = (f32[2,256]{1,0:T(2,128)S(1)}, f32[2,256]{1,0:T(2,128)S(1)}, u32[]{:S(2)}, u32[]{:S(2)}) collective-permute-start(f32[2,256]{1,0:T(2,128)S(1)} %slice.40), channel_id=1, source_target_pairs={{0,4},{4,8},{8,12},{12,16},{16,20},{20,24},{24,28},{28,32},{32,36}... | collective-permute-start | bytes 6152 | tf_op jit(solution)/shard_map/ppermute | solution.py:10
  12.3 0.8 slice_convert_fusion.2
  13.1 3.2 %convolution_convert_fusion.1 = bf16[384,2048]{1,0:T(8,128)(2,1)} fusion(bf16[256,2048]{1,0:T(8,128)(2,1)} %param.20, f32[2,256]{1,0:T(2,128)S(1)} %collective-permute-done, f32[384,256]{1,0:T(8,128)S(1)} %convert_multiply_fusion.2, bf16[384,256]{1,0:T(8,128)(2,1)} %param.16, f32[256]{0:T(256)S(1)} %bitcast.68, f32[256]{0:T(256)S(1)} %bitcast.69, ...), kind=kOutput, calls=%fused_computation.5 | convolution fusion | flops 404422656 | bytes 3216384 | tf_op jit(solution)/shard_map/dot_general | solution.py:64
  16.3 0.0 reduce-scatter.4.cloned.1.call-update
  16.3 0.0 all-gather.6.cloned.1.call-start
  16.3 0.6 copy-done.6
  16.9 0.1 copy.34
  17.1 0.2 reshape.92
  17.3 2.4 reduce-window.6
  19.7 0.1 slice.43
  19.9 0.1 copy.36
  20.0 0.1 reshape.129
  20.2 0.1 bitcast_bitcast_fusion
  20.3 0.1 fusion.26
  20.4 1.2 scatter_custom_fusion
  21.6 26.1 %reduce-scatter.4.cloned.1.call-done = bf16[96,2048]{1,0:T(8,128)(2,1)} async-done(((bf16[384,2048]{1,0:T(8,128)(2,1)}), bf16[96,2048]{1,0:T(8,128)(2,1)}) %reduce-scatter.4.cloned.1.call-update) | async-done | bytes 393232 | tf_op jit(solution)/shard_map/reduce_scatter | solution.py:63
  47.8 1.2 fusion.7
  49.0 1.2 fusion.9
  50.2 0.7 copy-done.3
  50.9 1.4 gather_fusion
  52.3 0.4 reshape.96
  52.8 39.5 %all_to_all.10 = bf16[64,4,2048]{2,1,0:T(4,128)(2,1)S(1)} all-to-all(bf16[64,4,2048]{2,1,0:T(4,128)(2,1)S(1)} %reshape.96), channel_id=1, replica_groups=mesh['sp'=64,'tp'=4] {'sp'}, dimensions={0} | all-to-all | bytes 2097152 | tf_op jit(solution)/shard_map/all_to_all | solution.py:85
  92.2 1.6 copy.39
  93.8 0.0 all-gather.6.cloned.1.call-update
  93.9 0.0 all-gather.4.cloned.1.call-start
  93.9 0.7 all-gather.4.cloned.1.call-update
  94.6 0.0 reduce-scatter.8.cloned.1.call-start
  94.7 45.3 %all-gather.6.cloned.1.call-done = bf16[64,16,2048]{2,0,1:T(8,128)(2,1)} async-done(((bf16[64,4,2048]{2,0,1:T(8,128)(2,1)}), bf16[64,16,2048]{2,0,1:T(8,128)(2,1)}) %all-gather.6.cloned.1.call-update) | async-done | bytes 4194320 | tf_op jit(solution)/shard_map/all_gather | solution.py:88
  140.0 3.6 %convolution_bitcast_fusion.1 = f32[64,1,16,256]{3,0,2,1:T(8,128)S(1)} fusion(bf16[64,16,2048]{2,0,1:T(8,128)(2,1)} %all-gather.6.cloned.1.call-done, bf16[1,2048,256]{2,1,0:T(8,128)(2,1)S(1)} %copy-done.9), kind=kOutput, calls=%fused_computation.9 | convolution fusion | flops 1073741824 | bytes 6291456 | tf_op jit(solution)/shard_map/gerd,edf->gerf/dot_general | solution.py:91
  143.6 1.3 fusion.2
  144.9 1.4 convert_bitcast_fusion
  146.3 4.2 %copy.41 = bf16[64,1,16,2048]{3,0,1,2:T(8,128)(2,1)} copy(bf16[64,1,16,2048]{3,2,0,1:T(8,128)(2,1)S(1)} %convert_bitcast_fusion) | data formatting | bytes 8388608 | tf_op jit(solution)/shard_map/optimization_barrier | solution.py:14
  150.6 0.2 reduce-scatter.6.cloned.1.call-start
  150.8 20.4 %all-gather.4.cloned.1.call-done = bf16[384,2048]{1,0:T(8,128)(2,1)} async-done(((bf16[96,2048]{1,0:T(8,128)(2,1)}), bf16[384,2048]{1,0:T(8,128)(2,1)}) %all-gather.4.cloned.1.call-update) | async-done | bytes 1572880 | tf_op jit(solution)/shard_map/all_gather | solution.py:89
  171.2 2.4 fusion.38
  173.6 4.5 %convolution_convert_fusion = bf16[384,2048]{1,0:T(8,128)(2,1)} fusion(bf16[256,2048]{1,0:T(8,128)(2,1)} %param.29, bf16[384,2048]{1,0:T(8,128)(2,1)S(1)} %copy-done.8, bf16[2048,256]{1,0:T(8,128)(2,1)} %param.28, f32[384,256]{1,0:T(8,128)S(1)} %fusion.38), kind=kOutput, calls=%fused_computation.4 | convolution fusion | flops 806682624 | bytes 5636096 | tf_op jit(solution)/shard_map/dot_general | solution.py:103
  178.2 44.9 %reduce-scatter.8.cloned.1.call-done = bf16[64,1,4,2048]{3,0,1,2:T(8,128)(2,1)} async-done(((bf16[64,1,16,2048]{3,0,1,2:T(8,128)(2,1)}), bf16[64,1,4,2048]{3,0,1,2:T(8,128)(2,1)}) %reduce-scatter.8.cloned.1.call-update) | async-done | bytes 1048592 | tf_op jit(solution)/shard_map/reduce_scatter | solution.py:106
  223.1 3.0 %copy.42 = bf16[64,1,4,2048]{3,2,1,0:T(4,128)(2,1)} copy(bf16[64,1,4,2048]{3,0,1,2:T(8,128)(2,1)} %reduce-scatter.8.cloned.1.call-done) | data formatting | bytes 2097152 | tf_op jit(solution)/shard_map/reduce_scatter | solution.py:106
  226.1 10.8 %all-to-all-start.1 = ((bf16[64,1,4,2048]{3,2,1,0:T(4,128)(2,1)}), bf16[64,1,4,2048]{3,2,1,0:T(4,128)(2,1)S(1)}, u32[]{:S(2)}, u32[]{:S(2)}) async-start(bf16[64,1,4,2048]{3,2,1,0:T(4,128)(2,1)} %copy.42), calls=%async_computation.4 | async-start | bytes 2097152 | tf_op jit(solution)/shard_map/all_to_all | solution.py:113
  236.9 0.8 constant_dynamic-slice_fusion
  237.7 0.7 copy.43
  238.4 26.7 %all-to-all-done.1 = bf16[64,1,4,2048]{3,2,1,0:T(4,128)(2,1)S(1)} async-done(((bf16[64,1,4,2048]{3,2,1,0:T(4,128)(2,1)}), bf16[64,1,4,2048]{3,2,1,0:T(4,128)(2,1)S(1)}, u32[]{:S(2)}, u32[]{:S(2)}) %all-to-all-start.1) | async-done | bytes 1048608 | tf_op jit(solution)/shard_map/all_to_all | solution.py:113
  265.1 0.3 reshape.103
  265.3 2.0 gather_fusion.1
  267.4 2.2 reshape.108
  269.6 3.2 %multiply_reduce_fusion = f32[96,2048]{1,0:T(8,128)} fusion(f32[96,2,2048]{2,1,0:T(2,128)S(1)} %reshape.108, f32[96,2]{1,0:T(8,128)S(1)} %copy-done.4), kind=kLoop, calls=%fused_computation.6 | loop fusion | flops 589824 | bytes 2360064 | tf_op jit(solution)/shard_map/reduce_sum | solution.py:119
  272.7 2.2 fusion.11
  (38 shorter events, 0.2 us)
Async XLA Ops:
  6.5 138.4 %copy-start = (bf16[1,256,2048]{2,1,0:T(8,128)(2,1)S(1)}, bf16[1,256,2048]{2,1,0:T(8,128)(2,1)}, u32[]{:S(2)}) copy-start(bf16[1,256,2048]{2,1,0:T(8,128)(2,1)} %param.26) | copy-start | bytes 3145732
  6.5 41.2 %reduce-scatter.4.cloned.1.call-start = ((), (), s32[]{:S(2)}) async-start(), calls=%async_computation.5 | async-start | bytes 1966080 | tf_op jit(solution)/shard_map/reduce_scatter | solution.py:63
  7.7 5.4 %collective-permute-start = (f32[2,256]{1,0:T(2,128)S(1)}, f32[2,256]{1,0:T(2,128)S(1)}, u32[]{:S(2)}, u32[]{:S(2)}) collective-permute-start(f32[2,256]{1,0:T(2,128)S(1)} %slice.40), channel_id=1, source_target_pairs={{0,4},{4,8},{8,12},{12,16},{16,20},{20,24},{24,28},{28,32},{32,36}... | collective-permute-start | bytes 6152 | tf_op jit(solution)/shard_map/ppermute | solution.py:10
  16.3 0.7 copy-start.6
  16.3 31.5 %copy-start.1 = (bf16[96,2048]{1,0:T(8,128)(2,1)S(1)}, bf16[96,2048]{1,0:T(8,128)(2,1)}, u32[]{:S(2)}) copy-start(bf16[96,2048]{1,0:T(8,128)(2,1)} %param.15) | copy-start | bytes 1179652
  16.3 123.7 %all-gather.6.cloned.1.call-start = ((), (), s32[]{:S(2)}) async-start(), calls=%async_computation.9 | async-start | bytes 5242880 | tf_op jit(solution)/shard_map/all_gather | solution.py:88
  17.3 31.7 %copy-start.5 = (f32[2048]{0:T(1024)S(1)}, f32[2048]{0:T(1024)}, u32[]{:S(2)}) copy-start(f32[2048]{0:T(1024)} %param.21) | copy-start | bytes 24580
  50.2 0.7 copy-start.3
  92.2 47.8 %copy-start.9 = (bf16[1,2048,256]{2,1,0:T(8,128)(2,1)S(1)}, bf16[1,2048,256]{2,1,0:T(8,128)(2,1)}, u32[]{:S(2)}) copy-start(bf16[1,2048,256]{2,1,0:T(8,128)(2,1)} %param.24) | copy-start | bytes 3145732
  93.9 77.3 %all-gather.4.cloned.1.call-start = ((), (), s32[]{:S(2)}) async-start(), calls=%async_computation.6 | async-start | bytes 1966080 | tf_op jit(solution)/shard_map/all_gather | solution.py:89
  94.6 49.0 %copy-start.10 = (bf16[1,2048,256]{2,1,0:T(8,128)(2,1)S(1)}, bf16[1,2048,256]{2,1,0:T(8,128)(2,1)}, u32[]{:S(2)}) copy-start(bf16[1,2048,256]{2,1,0:T(8,128)(2,1)} %param.25) | copy-start | bytes 3145732
  94.6 128.5 %reduce-scatter.8.cloned.1.call-start = ((), (), s32[]{:S(2)}) async-start(), calls=%async_computation.8 | async-start | bytes 5242880 | tf_op jit(solution)/shard_map/reduce_scatter | solution.py:106
  140.0 3.6 %copy-start.7 = (bf16[64,16,2048]{2,0,1:T(8,128)(2,1)S(1)}, bf16[64,16,2048]{2,0,1:T(8,128)(2,1)}, u32[]{:S(2)}) copy-start(bf16[64,16,2048]{2,0,1:T(8,128)(2,1)} %all-gather.6.cloned.1.call-done) | copy-start | bytes 12582916
  150.6 122.2 %reduce-scatter.6.cloned.1.call-start = ((), (), s32[]{:S(2)}) async-start(), calls=%async_computation.7 | async-start | bytes 1966080 | tf_op jit(solution)/shard_map/reduce_scatter | solution.py:109
  171.2 2.4 copy-start.8
  226.1 38.9 %all-to-all-start.1 = ((bf16[64,1,4,2048]{3,2,1,0:T(4,128)(2,1)}), bf16[64,1,4,2048]{3,2,1,0:T(4,128)(2,1)S(1)}, u32[]{:S(2)}, u32[]{:S(2)}) async-start(bf16[64,1,4,2048]{3,2,1,0:T(4,128)(2,1)} %copy.42), calls=%async_computation.4 | async-start | bytes 2097152 | tf_op jit(solution)/shard_map/all_to_all | solution.py:113
  267.4 2.2 copy-start.4
  269.5 3.2 %copy-start.2 = (bf16[96,2048]{1,0:T(8,128)(2,1)S(1)}, bf16[96,2048]{1,0:T(8,128)(2,1)}, u32[]{:S(2)}) copy-start(bf16[96,2048]{1,0:T(8,128)(2,1)} %reduce-scatter.4.cloned.1.call-done) | copy-start | bytes 1179652
Sparse Core Ops, SparseCore 0:
  16.4 31.3 reduce-scatter.3
  94.0 45.9 all-gather.5
  141.8 29.3 all-gather.3
  173.6 49.4 reduce-scatter.7
  225.5 27.2 reduce-scatter.5
where the time goes:
time: 282 us; the launch traced here: 281 us
  waiting for transfers between devices  164 us (58%)
  blocking collectives  39.5 us (14%)
  local copies, waits for them, and re-layouts  19.9 us (7%)
  matrix products  16.3 us (6%)
  starting transfers between devices  15.7 us (6%)
  between operations  13.4 us (5%)
  other arithmetic  12.4 us (4%)
    all_gather x1, waiting for transfers between devices, local(): lax.all_gather(arrived, 'tp', axis=2, tiled=True)  45.3 us
    reduce_scatter x1, waiting for transfers between devices, local(): lax.psum_scatter(partial_rows.astype(jnp.bfloat16), 'tp', scatter_dimensi...  44.9 us
    all_to_all x1, blocking collectives, local(): lax.all_to_all(outgoing, 'sp', split_axis=0, concat_axis=0, tiled=True)  39.5 us
    all_to_all x1, waiting for transfers between devices, local(): lax.all_to_all(summed.astype(jnp.bfloat16), 'sp', split_axis=0, concat_ax...  26.7 us
    reduce_scatter x1, waiting for transfers between devices, local(): lax.psum_scatter(round_trip(jnp.dot(mixed_rows, out_weight, preferred_ele...  26.1 us
    all_gather x1, waiting for transfers between devices, local(): lax.all_gather(normed, 'tp', axis=0, tiled=True)  20.4 us
    all_to_all x1, starting transfers between devices, local(): lax.all_to_all(summed.astype(jnp.bfloat16), 'sp', split_axis=0, concat_ax...  10.8 us
  transfers between devices with their start and end apart: 7, of which 5 were waited for; matrix products, arithmetic and copies ran while one was open for 12% of the time, Pallas kernels for 0%

commit v1 on v0

v1 whole, which is shorter than its diff:
```python
import functools

import jax
import jax.numpy as jnp
from jax import lax
from jax.experimental import pallas as pl
from jax.experimental.pallas import tpu as pltpu
from jax.sharding import PartitionSpec as P

F32 = jnp.float32
BF16 = jnp.bfloat16
CAP = 4
TP = 4


def remote(src, dst, send_sem, recv_sem, sp, tp):
    return pltpu.make_async_remote_copy(
        src_ref=src,
        dst_ref=dst,
        send_sem=send_sem,
        recv_sem=recv_sem,
        device_id=(sp, tp),
        device_id_type=pl.DeviceIdType.MESH,
    )


def add_into(dst, src):
    dst[...] = (dst[...].astype(F32) + src[...].astype(F32)).astype(BF16)


def kernel(
    groups,
    resid_h, cb_h, cc_h, cx_h, taps, ow_h, gain, routes, rweight,
    wg_h, wu_h, wd_h, sg_h, su_h, sd_h,
    out,
    resid, cb, cc, cx, ow, wg, wu, wd, sg, su, sd,
    prod, mixed, halo, own, proj, proj1, proj2, mid, nrm,
    part, part1, part2,
    disp, wcomb, outgoing, arr, res, res1, res2, summed, ret,
    load_sem, halo_sem, proj_s, proj_r, nrm_s, nrm_r, part_s, part_r,
    a2a_s, a2a_r, ag_s, ag_r, rs_s, rs_r, back_s, back_r,
):
    s = lax.axis_index("sp")
    x = lax.axis_index("tp")
    sp_count = lax.axis_size("sp")
    zs = sp_count // groups
    half = groups // 2
    q, d_model = resid.shape
    dh = d_model // 2
    right = lax.rem(x + 1, TP)
    left = lax.rem(x + TP - 1, TP)
    z = lax.div(s, groups)
    g = lax.rem(s, groups)

    def sp_ahead(dz, dg):
        return lax.rem(z + dz, zs) * groups + lax.rem(g + dg, groups)

    def sp_behind(dz, dg):
        return lax.rem(z + zs - dz, zs) * groups + lax.rem(g + groups - dg, groups)

    def zone(i):
        k = lax.div(i + 1, 2)
        return lax.rem(zs // 2 + zs + (1 - 2 * lax.rem(i, 2)) * k, zs)

    pairs = (
        (cb_h, cb), (cc_h, cc), (cx_h, cx), (ow_h, ow), (resid_h, resid),
        (wg_h.at[0], wg), (wu_h.at[0], wu), (wd_h.at[0], wd), (sg_h, sg), (su_h, su), (sd_h, sd),
    )
    loads = [pltpu.make_async_copy(a, b, load_sem.at[i]) for i, (a, b) in enumerate(pairs)]
    for one in loads:
        one.start()

    barrier = pltpu.get_barrier_semaphore()

    @pl.loop(1, sp_count)
    def _(d):
        pl.semaphore_signal(
            barrier, inc=1, device_id=(lax.rem(s + d, sp_count), x),
            device_id_type=pl.DeviceIdType.MESH,
        )

    for side in (right, left):
        pl.semaphore_signal(
            barrier, inc=1, device_id=(s, side), device_id_type=pl.DeviceIdType.MESH
        )

    slots = sp_count * CAP
    i_slot = lax.broadcasted_iota(jnp.int32, (q, slots), 1)
    rank = lax.rem(i_slot, CAP)
    offset = lax.div(i_slot, CAP)
    e_slot = lax.rem(lax.div(offset, groups) + z, zs) * groups + lax.rem(
        lax.rem(offset, groups) + g, groups
    )
    rows = pl.ds(x * q, q)
    route_0 = routes[rows, 0:1]
    route_1 = routes[rows, 1:2]
    is_0 = e_slot == route_0
    named = jnp.where(is_0 | (e_slot == route_1), 1.0, 0.0)
    before = lax.broadcasted_iota(jnp.int32, (q, q), 0) > lax.broadcasted_iota(
        jnp.int32, (q, q), 1
    )
    count = jnp.dot(
        jnp.where(before, 1.0, 0.0).astype(BF16), named.astype(BF16), preferred_element_type=F32
    )
    held = jnp.where(count == rank.astype(F32), named, 0.0)
    disp[...] = held.T.astype(BF16)
    weight = jnp.where(is_0, rweight[rows, 0:1], rweight[rows, 1:2]) * held
    weight_hi = weight.astype(BF16)
    wcomb[0] = weight_hi
    wcomb[1] = (weight - weight_hi.astype(F32)).astype(BF16)

    for i in range(3):
        loads[i].wait()
    toks = cc.shape[0]
    prod[8 : 8 + toks] = cc[...].astype(F32) * cx[...].astype(F32)
    halo[...] = prod[toks : toks + 8]
    pl.semaphore_wait(barrier, sp_count - 1 + 2)
    halo_copy = remote(
        halo, prod.at[0:8], halo_sem.at[0], halo_sem.at[1], lax.rem(s + 1, sp_count), x
    )
    halo_copy.start()
    loads[3].wait()
    loads[4].wait()
    halo_copy.wait_recv()
    first = jnp.where(s == 0, 0.0, 1.0)
    prod[0:8] = prod[0:8] * first
    conv = prod[6 : 6 + toks] * taps[0:1].astype(F32)
    conv = conv + prod[7 : 7 + toks] * taps[1:2].astype(F32)
    conv = conv + prod[8 : 8 + toks] * taps[2:3].astype(F32)
    mixed[...] = (cb[...].astype(F32) * conv).astype(BF16)

    def ring_sum(b, b1, b2, ssem, rsem):
        def begin():
            remote(b.at[2, 0], b1.at[0], ssem, rsem(0), s, right).start()
            remote(b.at[2, 1], b1.at[1], ssem, rsem(1), s, left).start()
            remote(b.at[3, 1], b2.at[0, 1], ssem, rsem(2), s, right).start()
            remote(b.at[1, 0], b2.at[1, 0], ssem, rsem(3), s, left).start()

        def turn():
            remote(b.at[2, 0], b1.at[0], ssem, rsem(0), s, left).wait_recv()
            add_into(b.at[3, 0], b1.at[0])
            remote(b.at[3, 0], b2.at[0, 0], ssem, rsem(4), s, right).start()
            remote(b.at[2, 1], b1.at[1], ssem, rsem(1), s, right).wait_recv()
            add_into(b.at[1, 1], b1.at[1])
            remote(b.at[1, 1], b2.at[1, 1], ssem, rsem(5), s, left).start()

        def finish():
            remote(b.at[3, 1], b2.at[0, 1], ssem, rsem(2), s, left).wait_recv()
            remote(b.at[1, 0], b2.at[1, 0], ssem, rsem(3), s, right).wait_recv()
            remote(b.at[3, 0], b2.at[0, 0], ssem, rsem(4), s, left).wait_recv()
            remote(b.at[1, 1], b2.at[1, 1], ssem, rsem(5), s, right).wait_recv()

        def drain():
            remote(b.at[0:3], b.at[0:3], ssem, rsem(0), s, right).wait_send()

        return begin, turn, finish, drain

    def ring_gather(b, ssem, rsem):
        def begin():
            remote(b.at[0], b.at[1], ssem, rsem(0), s, right).start()
            remote(b.at[0], b.at[3], ssem, rsem(1), s, left).start()

        def turn():
            remote(b.at[0], b.at[1], ssem, rsem(0), s, left).wait_recv()
            remote(b.at[1, 0], b.at[2, 0], ssem, rsem(2), s, right).start()
            remote(b.at[0], b.at[3], ssem, rsem(1), s, right).wait_recv()
            remote(b.at[3, 1], b.at[2, 1], ssem, rsem(3), s, left).start()

        def finish():
            remote(b.at[1, 0], b.at[2, 0], ssem, rsem(2), s, left).wait_recv()
            remote(b.at[3, 1], b.at[2, 1], ssem, rsem(3), s, right).wait_recv()

        def drain():
            remote(b.at[0:3], b.at[0:3], ssem, rsem(0), s, right).wait_send()

        return begin, turn, finish, drain

    def project(j):
        block = lax.rem(x + TP - j, TP)
        return mixed[pl.ds(pl.multiple_of(block * q, 16), q)]

    proj_begin, proj_turn, proj_finish, proj_drain = ring_sum(
        proj, proj1, proj2, proj_s, lambda k: proj_r.at[k]
    )
    for j in (2, 3, 1):
        for h in range(2):
            proj[j, h] = jnp.dot(
                project(j), ow[:, h * dh : (h + 1) * dh], preferred_element_type=F32
            ).astype(BF16)
    proj_begin()
    for h in range(2):
        own[h] = jnp.dot(project(0), ow[:, h * dh : (h + 1) * dh], preferred_element_type=F32)
    proj_turn()
    proj_finish()
    square = jnp.zeros((q, 1), F32)
    for h in range(2):
        total = own[h] + proj2[0, h].astype(F32) + proj2[1, h].astype(F32)
        m = (resid[:, h * dh : (h + 1) * dh].astype(F32) + total).astype(BF16)
        mid[h] = m
        m = m.astype(F32)
        square = square + jnp.sum(m * m, axis=-1, keepdims=True)
    scale = lax.rsqrt(square * (1.0 / d_model) + 1e-06)
    for h in range(2):
        nrm[0, h] = (mid[h].astype(F32) * scale * gain[:, h * dh : (h + 1) * dh]).astype(BF16)

    nrm_begin, nrm_turn, nrm_finish, nrm_drain = ring_gather(nrm, nrm_s, lambda k: nrm_r.at[k])
    nrm_begin()

    @pl.loop(0, zs)
    def _(i):
        dz = zone(i)
        table = disp[pl.ds(pl.multiple_of(dz * groups * CAP, groups * CAP), groups * CAP)]
        for h in range(2):
            picked = jnp.dot(table, nrm[0, h], preferred_element_type=F32)
            outgoing[dz, :, :, :, h * dh : (h + 1) * dh] = picked.astype(BF16).reshape(
                2, half, CAP, dh
            )
        for dg in range(groups):
            @pl.when((dz != 0) | (dg != 0))
            def _():
                remote(
                    outgoing.at[dz, dg // half, dg % half], arr.at[dz, 0, dg // half, dg % half],
                    a2a_s.at[dz], a2a_r.at[dz], sp_ahead(dz, dg), x,
                ).start()

    arr[0, 0, 0, 0] = outgoing[0, 0, 0]
    for one in loads[5:]:
        one.wait()
    nrm_turn()

    def chain(dz):
        return ring_sum(
            res.at[dz], res1.at[dz], res2.at[dz], rs_s.at[dz], lambda k: rs_r.at[dz, k]
        )

    def spread(dz):
        return ring_gather(arr.at[dz], ag_s.at[dz], lambda k: ag_r.at[dz, k])

    some = ret.at[0 : groups - 1, 0, 0]
    n_rows = TP * groups * CAP
    kc = min(256, d_model)
    nc = min(512, dh)

    def expert(dz):
        gate = jnp.zeros((n_rows, wg.shape[1]), F32)
        up = jnp.zeros((n_rows, wg.shape[1]), F32)
        for k in range(d_model // kc):
            cols = slice(k * kc, (k + 1) * kc)
            block = arr[dz, :, :, :, :, cols].reshape(n_rows, kc)
            gate = gate + jnp.dot(block, wg[cols], preferred_element_type=F32)
            up = up + jnp.dot(block, wu[cols], preferred_element_type=F32)
        hidden = (jax.nn.silu(gate) * up).astype(BF16)
        for n in range(d_model // nc):
            cols = slice(n * nc, (n + 1) * nc)
            res[dz, :, :, :, :, cols] = (
                jnp.dot(hidden, wd[:, cols], preferred_element_type=F32)
                .astype(BF16)
                .reshape(TP, 2, half, CAP, nc)
            )

    part_begin, part_turn, part_finish, part_drain = ring_sum(
        part, part1, part2, part_s, lambda k: part_r.at[k]
    )

    def shared():
        gate = jnp.zeros((TP * q, sg.shape[1]), F32)
        up = jnp.zeros((TP * q, sg.shape[1]), F32)
        for h in range(2):
            block = nrm[:, h].reshape(TP * q, dh)
            gate = gate + jnp.dot(block, sg[h * dh : (h + 1) * dh], preferred_element_type=F32)
            up = up + jnp.dot(block, su[h * dh : (h + 1) * dh], preferred_element_type=F32)
        hidden = (jax.nn.silu(gate) * up).astype(BF16)
        for h in range(2):
            part[:, h] = (
                jnp.dot(hidden, sd[:, h * dh : (h + 1) * dh], preferred_element_type=F32)
                .astype(BF16)
                .reshape(TP, q, dh)
            )

    @pl.loop(0, zs + 4)
    def _(i):
        @pl.when(i < zs)
        def _():
            dz = zone(i)
            wait_zone(arr.at[dz, 0], some, dz, a2a_s, a2a_r, True, s, right)
            spread(dz)[0]()

        @pl.when((i >= 1) & (i < zs + 1))
        def _():
            spread(zone(i - 1))[1]()

        @pl.when(i == 1)
        def _():
            nrm_finish()
            shared()
            part_begin()

        @pl.when((i >= 2) & (i < zs + 2))
        def _():
            dz = zone(i - 2)
            spread(dz)[2]()
            expert(dz)
            chain(dz)[0]()

        @pl.when(i == 2)
        def _():
            part_turn()

        @pl.when((i >= 3) & (i < zs + 3))
        def _():
            chain(zone(i - 3))[1]()

        @pl.when(i >= 4)
        def _():
            dz = zone(i - 4)
            chain(dz)[2]()
            summed[dz] = (
                res[dz, 0].astype(F32) + res2[dz, 0].astype(F32) + res2[dz, 1].astype(F32)
            ).astype(BF16)
            for dg in range(groups):
                @pl.when((dz != 0) | (dg != 0))
                def _():
                    remote(
                        summed.at[dz, dg // half, dg % half], ret.at[dz, dg // half, dg % half],
                        back_s.at[dz], back_r.at[dz], sp_behind(dz, dg), x,
                    ).start()

    ret[0, 0, 0] = summed[0, 0, 0]
    part_finish()

    @pl.loop(0, zs)
    def _(i):
        dz = zone(i)
        wait_zone(ret.at[dz], some, dz, back_s, back_r, True, s, right)

    for n in range(d_model // nc):
        h, c = divmod(n * nc, dh)
        cols = slice(n * nc, (n + 1) * nc)
        local = slice(c, c + nc)
        block = ret[:, :, :, :, cols].reshape(slots, nc)
        total = jnp.dot(wcomb[0], block, preferred_element_type=F32)
        total = total + jnp.dot(wcomb[1], block, preferred_element_type=F32)
        total = total + part[0, h, :, local].astype(F32)
        total = total + part2[0, h, :, local].astype(F32) + part2[1, h, :, local].astype(F32)
        out[:, cols] = (mid[h, :, local].astype(F32) + total).astype(BF16)

    halo_copy.wait_send()
    proj_drain()
    nrm_drain()
    part_drain()

    @pl.loop(0, zs)
    def _(dz):
        wait_zone(outgoing.at[dz], some, dz, a2a_s, a2a_r, False, s, right)
        wait_zone(summed.at[dz], some, dz, back_s, back_r, False, s, right)
        spread(dz)[3]()
        chain(dz)[3]()


def wait_zone(ref, some, dz, ssem, rsem, recv, s, right):
    def fire(a):
        one = remote(a, a, ssem.at[dz], rsem.at[dz], s, right)
        if recv:
            one.wait_recv()
        else:
            one.wait_send()

    @pl.when(dz != 0)
    def _():
        fire(ref)

    @pl.when(dz == 0)
    def _():
        fire(some)


def local(
    resid, conv_b, conv_c, conv_x, conv_taps, out_weight, norm_gain, routes, route_weight,
    expert_gate, expert_up, expert_down, shared_gate, shared_up, shared_down,
):
    sp_count = lax.axis_size("sp")
    groups = max(2, sp_count // 8)
    zs = sp_count // groups
    half = groups // 2
    q, d = resid.shape
    toks, ch = conv_b.shape
    ff = expert_gate.shape[2]
    dh = d // 2
    vmem = pltpu.VMEM
    dma = pltpu.SemaphoreType.DMA
    anywhere = pl.BlockSpec(memory_space=pl.ANY)
    inside = pl.BlockSpec(memory_space=pltpu.VMEM)
    return pl.pallas_call(
        functools.partial(kernel, groups),
        out_shape=jax.ShapeDtypeStruct((q, d), BF16),
        in_specs=[anywhere] * 4 + [inside, anywhere] + [inside] * 3 + [anywhere] * 6,
        out_specs=inside,
        scratch_shapes=[
            vmem((q, d), BF16), vmem((toks, ch), BF16), vmem((toks, ch), BF16),
            vmem((toks, ch), BF16), vmem((ch, d), BF16),
            vmem((d, ff), BF16), vmem((d, ff), BF16), vmem((ff, d), BF16),
            vmem((d, ff), BF16), vmem((d, ff), BF16), vmem((ff, d), BF16),
            vmem((toks + 8, ch), F32), vmem((toks, ch), BF16), vmem((8, ch), F32),
            vmem((2, q, dh), F32),
            vmem((4, 2, q, dh), BF16), vmem((2, q, dh), BF16), vmem((2, 2, q, dh), BF16),
            vmem((2, q, dh), BF16), vmem((4, 2, q, dh), BF16),
            vmem((4, 2, q, dh), BF16), vmem((2, q, dh), BF16), vmem((2, 2, q, dh), BF16),
            vmem((sp_count * CAP, q), BF16), vmem((2, q, sp_count * CAP), BF16),
            vmem((zs, 2, half, CAP, d), BF16),
            vmem((zs, 4, 2, half, CAP, d), BF16),
            vmem((zs, 4, 2, half, CAP, d), BF16),
            vmem((zs, 2, half, CAP, d), BF16),
            vmem((zs, 2, 2, half, CAP, d), BF16),
            vmem((zs, 2, half, CAP, d), BF16),
            vmem((zs, 2, half, CAP, d), BF16),
            dma((11,)), dma((2,)), dma(()), dma((6,)), dma(()), dma((4,)), dma(()), dma((6,)),
            dma((zs,)), dma((zs,)), dma((zs,)), dma((zs, 4)), dma((zs,)), dma((zs, 6)),
            dma((zs,)), dma((zs,)),
        ],
        compiler_params=pltpu.CompilerParams(
            collective_id=0, has_side_effects=True, vmem_limit_bytes=60 * 1024 * 1024
        ),
        name="layer",
    )(
        resid, conv_b, conv_c, conv_x, conv_taps, out_weight, norm_gain.reshape(1, d), routes,
        route_weight, expert_gate, expert_up, expert_down, shared_gate, shared_up, shared_down,
    )


def solution(mesh):
    return jax.shard_map(
        local,
        mesh=mesh,
        in_specs=(
            P(("sp", "tp"), None),
            P("sp", "tp"),
            P("sp", "tp"),
            P("sp", "tp"),
            P(None, "tp"),
            P("tp", None),
            P(),
            P("sp", None),
            P("sp", None),
            P("sp", None, "tp"),
            P("sp", None, "tp"),
            P("sp", "tp", None),
            P(None, "tp"),
            P(None, "tp"),
            P("tp", None),
        ),
        out_specs=P(("sp", "tp"), None),
        check_vma=False,
    )
```

time: 282 us -> 139 us (0.49)
  waiting for transfers between devices: 164 us -> 0 us
  Pallas kernels: 0 us -> 135 us
  blocking collectives: 39.5 us -> 0 us
  matrix products: 16.3 us -> 0 us
  local copies, waits for them, and re-layouts: 19.9 us -> 4.12 us
  starting transfers between devices: 15.7 us -> 0 us
  between operations: 13.4 us -> 0.01 us
  other arithmetic: 12.4 us -> 0 us
    pallas_call x0 -> x1, Pallas kernels: none -> 135 us  [local(): pl.pallas_call(functools.partial(kernel, groups), out_shape=jax.ShapeDtyp...]
    reduce_scatter x3 -> x0, waiting for transfers between devices: 71.1 us -> none  [the longest x1 44.9 us: local(): lax.psum_scatter(partial_rows.astype(jnp.bfloat16), 'tp', scatter_dimensi...]
    all_gather x2 -> x0, waiting for transfers between devices: 65.8 us -> none  [the longest x1 45.3 us: local(): lax.all_gather(arrived, 'tp', axis=2, tiled=True)]
    all_to_all x1 -> x0, blocking collectives: 39.5 us -> none  [local(): lax.all_to_all(outgoing, 'sp', split_axis=0, concat_axis=0, tiled=True)]
    all_to_all x1 -> x0, waiting for transfers between devices: 26.7 us -> none  [local(): lax.all_to_all(summed.astype(jnp.bfloat16), 'sp', split_axis=0, concat_ax...]
    dot_general x6 -> x0, matrix products: 16.3 us -> none  [the longest x1 4.52 us: local(): jnp.dot(shared_hidden, shared_down, preferred_element_type=jnp.float32)]
    all_to_all x1 -> x0, starting transfers between devices: 10.8 us -> none  [local(): lax.all_to_all(summed.astype(jnp.bfloat16), 'sp', split_axis=0, concat_ax...]
    ppermute x1 -> x0, starting transfers between devices: 4.58 us -> none  [shifted(): return lax.ppermute(block, axis, route)]
  transfers between devices with their start and end apart: 7 -> 0, of which waited for: 5 -> 0; matrix products, arithmetic and copies ran while one was open for 12% -> 0% of each run, Pallas kernels for 0% -> 0%
where the time goes in v1:
time: 139 us
  Pallas kernels  135 us (97%)
  local copies, waits for them, and re-layouts  4.12 us (3%)
    pallas_call x1, Pallas kernels, local(): pl.pallas_call(functools.partial(kernel, groups), out_shape=jax.ShapeDtyp...  135 us
    unnamed x5, local copies, waits for them, and re-layouts  4.12 us

profile of v1, /device:TPU:1, one launch (start us, length us, event | category | flops | bytes accessed | tf_op | source)
XLA Modules:
  0.0 139.2 jit_solution(18232792975666975855)
XLA Ops:
  0.0 0.0 copy-start
  0.0 1.5 %copy.16.routes = s32[384,2]{1,0:T(8,128)} copy(s32[384,2]{0,1:T(2,128)} %param.22) | data formatting | bytes 6144 | tf_op args[7]
  1.5 0.0 copy-done
  1.5 0.8 copy.17.rweight
  2.4 135.1 %layer.1 = bf16[96,2048]{1,0:T(8,128)(2,1)} custom-call(bf16[96,2048]{1,0:T(8,128)(2,1)} %resid_h.1, bf16[384,256]{1,0:T(8,128)(2,1)} %cb_h.1, bf16[384,256]{1,0:T(8,128)(2,1)} %cc_h.1, bf16[384,256]{1,0:T(8,128)(2,1)} %cx_h.1, bf16[3,256]{1,0:T(4,128)(2,1)} %taps.1, bf16[256,2048]{1,0:T(8,128)(2,1)} %ow_h.1, f32[1,2048]{1,0:T(1,128)} %bitcast.1, ...), custom_call_target="tpu_custom_call" | custom-call | tf_op jit(solution)/shard_map/layer/pallas_call | solution.py:393
  137.4 1.8 %copy.19 = bf16[96,2048]{1,0:T(8,128)(2,1)} copy(bf16[96,2048]{1,0:T(8,128)(2,1)} %layer.1) | data formatting | bytes 786432
Async XLA Ops:
  0.0 1.5 %copy-start = (f32[384,2]{0,1:T(2,128)S(1)}, f32[384,2]{0,1:T(2,128)}, u32[]{:S(2)}) copy-start(f32[384,2]{0,1:T(2,128)} %param.23) | copy-start | bytes 9220

commit v2 on v1

v2 whole, which is shorter than its diff:
```python
import functools

import jax
import jax.numpy as jnp
from jax import lax
from jax.experimental import pallas as pl
from jax.experimental.pallas import tpu as pltpu
from jax.sharding import PartitionSpec as P

F32 = jnp.float32
BF16 = jnp.bfloat16
CAP = 4
TP = 4
NEAR = 3


def remote(src, dst, send_sem, recv_sem, sp, tp):
    return pltpu.make_async_remote_copy(
        src_ref=src,
        dst_ref=dst,
        send_sem=send_sem,
        recv_sem=recv_sem,
        device_id=(sp, tp),
        device_id_type=pl.DeviceIdType.MESH,
    )


def add_into(dst, src):
    dst[...] = (dst[...].astype(F32) + src[...].astype(F32)).astype(BF16)


def kernel(
    groups,
    resid_h, cb_h, cc_h, cx_h, taps, ow_h, gain, routes, rweight,
    wg_h, wu_h, wd_h, sg_h, su_h, sd_h,
    out,
    resid, cb, cc, cx, ow, wg, wu, wd, sg, su, sd,
    prod, mixed, halo, halo_in, own, proj, proj1, proj2, mid, nrm,
    part, part1, part2, partf,
    rowform, colform, disp, wcomb, outgoing, arr, res, res1, res2, summed, ret,
    near_disp, near_w, near_out, near_arr, near_res, near_ret,
    load_sem, halo_sem, proj_s, proj_r, nrm_s, nrm_r, part_s, part_r,
    a2a_s, a2a_r, ag_s, ag_r, rs_s, rs_r, back_s, back_r, out_s, out_r, home_s, home_r,
):
    s = lax.axis_index("sp")
    x = lax.axis_index("tp")
    sp_count = lax.axis_size("sp")
    zs = sp_count // groups
    far = zs - NEAR
    half = groups // 2
    q, d_model = resid.shape
    dh = d_model // 2
    toks = cc.shape[0]
    msg = TP * CAP
    right = lax.rem(x + 1, TP)
    left = lax.rem(x + TP - 1, TP)
    z = lax.div(s, groups)
    g = lax.rem(s, groups)

    def sp_ahead(dz, dg):
        return lax.rem(z + dz, zs) * groups + lax.rem(g + dg, groups)

    def sp_behind(dz, dg):
        return lax.rem(z + zs - dz, zs) * groups + lax.rem(g + groups - dg, groups)

    def zone(i):
        k = lax.div(i + 1, 2)
        return lax.rem(zs // 2 + zs + (1 - 2 * lax.rem(i, 2)) * k, zs)

    def near_zone(k):
        return jnp.where(k == 0, 1, jnp.where(k == 1, zs - 1, 0))

    pairs = (
        (cc_h, cc), (cx_h, cx), (cb_h, cb), (ow_h, ow), (resid_h, resid),
        (sg_h, sg), (su_h, su), (sd_h, sd), (wg_h.at[0], wg), (wu_h.at[0], wu), (wd_h.at[0], wd),
    )
    loads = [pltpu.make_async_copy(a, b, load_sem.at[i]) for i, (a, b) in enumerate(pairs)]
    for one in loads:
        one.start()

    barrier = pltpu.get_barrier_semaphore()

    for side in (right, left):
        pl.semaphore_signal(
            barrier, inc=1, device_id=(s, side), device_id_type=pl.DeviceIdType.MESH
        )

    @pl.loop(1, sp_count)
    def _(d):
        pl.semaphore_signal(
            barrier, inc=1, device_id=(lax.rem(s + d, sp_count), x),
            device_id_type=pl.DeviceIdType.MESH,
        )

    for i in range(3):
        loads[i].wait()
    prod[0:8] = jnp.zeros((8, prod.shape[1]), F32)
    prod[8 : 8 + toks] = cc[...].astype(F32) * cx[...].astype(F32)
    halo[...] = prod[toks : toks + 8]

    def mix(n):
        conv = prod[6 : 6 + n] * taps[0:1].astype(F32)
        conv = conv + prod[7 : 7 + n] * taps[1:2].astype(F32)
        conv = conv + prod[8 : 8 + n] * taps[2:3].astype(F32)
        mixed[0:n] = (cb[0:n].astype(F32) * conv).astype(BF16)

    def project(j):
        block = lax.rem(x + TP - j, TP)
        return mixed[pl.ds(pl.multiple_of(block * q, 16), q)]

    mix(toks)
    loads[3].wait()
    for j in (2, 3, 1):
        for h in range(2):
            proj[j, h] = jnp.dot(
                project(j), ow[:, h * dh : (h + 1) * dh], preferred_element_type=F32
            ).astype(BF16)

    pl.semaphore_wait(barrier, sp_count - 1 + 2)
    halo_copy = remote(
        halo, halo_in, halo_sem.at[0], halo_sem.at[1], lax.rem(s + 1, sp_count), x
    )
    halo_copy.start()

    def ring_sum(b, b1, b2, ssem, rsem):
        def begin():
            remote(b.at[2, 0], b1.at[0], ssem, rsem(0), s, right).start()
            remote(b.at[2, 1], b1.at[1], ssem, rsem(1), s, left).start()
            remote(b.at[3, 1], b2.at[0, 1], ssem, rsem(2), s, right).start()
            remote(b.at[1, 0], b2.at[1, 0], ssem, rsem(3), s, left).start()

        def turn():
            remote(b.at[2, 0], b1.at[0], ssem, rsem(0), s, left).wait_recv()
            add_into(b.at[3, 0], b1.at[0])
            remote(b.at[3, 0], b2.at[0, 0], ssem, rsem(4), s, right).start()
            remote(b.at[2, 1], b1.at[1], ssem, rsem(1), s, right).wait_recv()
            add_into(b.at[1, 1], b1.at[1])
            remote(b.at[1, 1], b2.at[1, 1], ssem, rsem(5), s, left).start()

        def finish():
            remote(b.at[3, 1], b2.at[0, 1], ssem, rsem(2), s, left).wait_recv()
            remote(b.at[1, 0], b2.at[1, 0], ssem, rsem(3), s, right).wait_recv()
            remote(b.at[3, 0], b2.at[0, 0], ssem, rsem(4), s, left).wait_recv()
            remote(b.at[1, 1], b2.at[1, 1], ssem, rsem(5), s, right).wait_recv()

        def drain():
            remote(b.at[0:3], b.at[0:3], ssem, rsem(0), s, right).wait_send()

        return begin, turn, finish, drain

    def ring_gather(b, ssem, rsem):
        def begin():
            remote(b.at[0], b.at[1], ssem, rsem(0), s, right).start()
            remote(b.at[0], b.at[3], ssem, rsem(1), s, left).start()

        def turn():
            remote(b.at[0], b.at[1], ssem, rsem(0), s, left).wait_recv()
            remote(b.at[1, 0], b.at[2, 0], ssem, rsem(2), s, right).start()
            remote(b.at[0], b.at[3], ssem, rsem(1), s, right).wait_recv()
            remote(b.at[3, 1], b.at[2, 1], ssem, rsem(3), s, left).start()

        def finish():
            remote(b.at[1, 0], b.at[2, 0], ssem, rsem(2), s, left).wait_recv()
            remote(b.at[3, 1], b.at[2, 1], ssem, rsem(3), s, right).wait_recv()

        def drain():
            remote(b.at[0:3], b.at[0:3], ssem, rsem(0), s, right).wait_send()

        return begin, turn, finish, drain

    proj_begin, proj_turn, proj_finish, proj_drain = ring_sum(
        proj, proj1, proj2, proj_s, lambda k: proj_r.at[k]
    )
    halo_copy.wait_recv()
    prod[0:8] = halo_in[...] * jnp.where(s == 0, 0.0, 1.0)
    mix(16)
    for h in range(2):
        proj[x, h, 0:16] = jnp.dot(
            mixed[0:16], ow[:, h * dh : (h + 1) * dh], preferred_element_type=F32
        ).astype(BF16)
    proj_begin()
    for h in range(2):
        own[h] = jnp.dot(project(0), ow[:, h * dh : (h + 1) * dh], preferred_element_type=F32)

    rowform[0:2] = routes[...].astype(F32)
    rowform[2:4] = rweight[...]
    colform[...] = rowform[...].T
    before = lax.broadcasted_iota(jnp.int32, (q, q), 0) > lax.broadcasted_iota(
        jnp.int32, (q, q), 1
    )
    earlier = jnp.where(before, 1.0, 0.0).astype(BF16)

    def table(j, dz, dg, rank, extra):
        expert = lax.rem(dz + z, zs) * groups + lax.rem(dg + g, groups)
        expert = expert.astype(F32)
        rows = pl.ds(pl.multiple_of(lax.rem(x + TP - j, TP) * q, 16), q)
        is_0 = expert == colform[rows, 0:1]
        named = jnp.where(is_0 | (expert == colform[rows, 1:2]), 1.0, 0.0)
        count = jnp.dot(earlier, named.astype(BF16), preferred_element_type=F32)
        held = jnp.where((count == rank.astype(F32)) & extra, named, 0.0)
        weight = jnp.where(is_0, colform[rows, 2:3], colform[rows, 3:4]) * held
        high = weight.astype(BF16)
        return held.T.astype(BF16), high, (weight - high.astype(F32)).astype(BF16)

    far_slots = far * groups * CAP
    i_slot = lax.broadcasted_iota(jnp.int32, (q, far_slots), 1)
    offset = lax.div(i_slot, CAP)
    disp[...], wcomb[0], wcomb[1] = table(
        0, zone(lax.div(offset, groups)), lax.rem(offset, groups), lax.rem(i_slot, CAP),
        i_slot >= 0,
    )

    proj_turn()

    near_slots = NEAR * groups * msg
    n_slot = lax.broadcasted_iota(jnp.int32, (q, near_slots), 1)
    near_offset = lax.div(n_slot, msg)
    for j in range(TP):
        near_disp[j], near_w[0, j], near_w[1, j] = table(
            j, near_zone(lax.div(near_offset, groups)), lax.rem(near_offset, groups),
            lax.rem(n_slot, CAP), lax.rem(lax.div(n_slot, CAP), TP) == j,
        )

    loads[4].wait()
    proj_finish()
    square = jnp.zeros((q, 1), F32)
    for h in range(2):
        total = own[h] + proj2[0, h].astype(F32) + proj2[1, h].astype(F32)
        m = (resid[:, h * dh : (h + 1) * dh].astype(F32) + total).astype(BF16)
        mid[h] = m
        m = m.astype(F32)
        square = square + jnp.sum(m * m, axis=-1, keepdims=True)
    scale = lax.rsqrt(square * (1.0 / d_model) + 1e-06)
    for h in range(2):
        nrm[0, h] = (mid[h].astype(F32) * scale * gain[:, h * dh : (h + 1) * dh]).astype(BF16)

    nrm_begin, nrm_turn, nrm_finish, nrm_drain = ring_gather(nrm, nrm_s, lambda k: nrm_r.at[k])
    nrm_begin()

    zone_rows = groups * CAP

    @pl.loop(0, far)
    def _(i):
        rows = disp[pl.ds(pl.multiple_of(i * zone_rows, zone_rows), zone_rows)]
        for h in range(2):
            picked = jnp.dot(rows, nrm[0, h], preferred_element_type=F32)
            outgoing[i, :, :, :, h * dh : (h + 1) * dh] = picked.astype(BF16).reshape(
                2, half, CAP, dh
            )
        for dg in range(groups):
            remote(
                outgoing.at[i, dg // half, dg % half], arr.at[i, 0, dg // half, dg % half],
                a2a_s.at[i], a2a_r.at[i], sp_ahead(zone(i), dg), x,
            ).start()

    for one in loads[5:]:
        one.wait()
    nrm_turn()
    nrm_finish()

    near_rows = groups * msg

    def near_send(src, dst, k, ssem, rsem, target):
        for dg in range(groups):
            @pl.when((k != NEAR - 1) | (dg != 0))
            def _():
                rows = slice(dg * msg, (dg + 1) * msg)
                remote(
                    src.at[k, rows], dst.at[k, rows], ssem.at[k], rsem.at[k],
                    target(near_zone(k), dg), x,
                ).start()

    def near_wait(ref, k, ssem, rsem, recv):
        def fire(a):
            one = remote(a, a, ssem.at[k], rsem.at[k], s, right)
            if recv:
                one.wait_recv()
            else:
                one.wait_send()

        @pl.when(k != NEAR - 1)
        def _():
            fire(ref.at[k])

        @pl.when(k == NEAR - 1)
        def _():
            fire(ref.at[k, msg:near_rows])

    @pl.loop(0, NEAR)
    def _(k):
        rows = pl.ds(pl.multiple_of(k * near_rows, near_rows), near_rows)
        for h in range(2):
            picked = jnp.dot(near_disp[0, rows], nrm[0, h], preferred_element_type=F32)
            for j in range(1, TP):
                picked = picked + jnp.dot(
                    near_disp[j, rows], nrm[j, h], preferred_element_type=F32
                )
            near_out[k, :, h * dh : (h + 1) * dh] = picked.astype(BF16)
        near_send(near_out, near_arr, k, out_s, out_r, sp_ahead)

    near_arr[NEAR - 1, 0:msg] = near_out[NEAR - 1, 0:msg]

    def chain(i):
        return ring_sum(res.at[i], res1.at[i], res2.at[i], rs_s.at[i], lambda k: rs_r.at[i, k])

    def spread(i):
        return ring_gather(arr.at[i], ag_s.at[i], lambda k: ag_r.at[i, k])

    n_rows = TP * groups * CAP
    kc = min(256, d_model)
    nc = min(512, dh)

    def expert(read, write):
        gate = jnp.zeros((n_rows, wg.shape[1]), F32)
        up = jnp.zeros((n_rows, wg.shape[1]), F32)
        for k in range(d_model // kc):
            cols = slice(k * kc, (k + 1) * kc)
            block = read(cols)
            gate = gate + jnp.dot(block, wg[cols], preferred_element_type=F32)
            up = up + jnp.dot(block, wu[cols], preferred_element_type=F32)
        hidden = (jax.nn.silu(gate) * up).astype(BF16)
        for n in range(d_model // nc):
            cols = slice(n * nc, (n + 1) * nc)
            write(cols, jnp.dot(hidden, wd[:, cols], preferred_element_type=F32).astype(BF16))

    def far_expert(i):
        def write(cols, value):
            res[i, :, :, :, :, cols] = value.reshape(TP, 2, half, CAP, nc)

        expert(lambda cols: arr[i, :, :, :, :, cols].reshape(n_rows, kc), write)

    def near_expert(k):
        def write(cols, value):
            near_res[k, :, cols] = value

        expert(lambda cols: near_arr[k, :, cols], write)

    part_begin, part_turn, part_finish, part_drain = ring_sum(
        part, part1, part2, part_s, lambda k: part_r.at[k]
    )

    def shared():
        gate = jnp.zeros((TP * q, sg.shape[1]), F32)
        up = jnp.zeros((TP * q, sg.shape[1]), F32)
        for h in range(2):
            block = nrm[:, h].reshape(TP * q, dh)
            gate = gate + jnp.dot(block, sg[h * dh : (h + 1) * dh], preferred_element_type=F32)
            up = up + jnp.dot(block, su[h * dh : (h + 1) * dh], preferred_element_type=F32)
        hidden = (jax.nn.silu(gate) * up).astype(BF16)
        for h in range(2):
            partf[:, h] = jnp.dot(
                hidden, sd[:, h * dh : (h + 1) * dh], preferred_element_type=F32
            ).reshape(TP, q, dh)

    def near_combine():
        for j in range(TP):
            for n in range(d_model // nc):
                h, c = divmod(n * nc, dh)
                block = near_ret[:, :, n * nc : (n + 1) * nc].reshape(near_slots, nc)
                total = partf[j, h, :, c : c + nc]
                total = total + jnp.dot(near_w[0, j], block, preferred_element_type=F32)
                total = total + jnp.dot(near_w[1, j], block, preferred_element_type=F32)
                part[j, h, :, c : c + nc] = total.astype(BF16)

    @pl.loop(0, STEPS(far))
    def _(i):
        @pl.when(i < far)
        def _():
            a = arr.at[i, 0]
            remote(a, a, a2a_s.at[i], a2a_r.at[i], s, right).wait_recv()
            spread(i)[0]()

        @pl.when((i >= 1) & (i < far + 1))
        def _():
            spread(i - 1)[1]()

        @pl.when(i == 1)
        def _():
            shared()

        @pl.when((i >= 2) & (i < far + 2))
        def _():
            spread(i - 2)[2]()
            far_expert(i - 2)
            chain(i - 2)[0]()

        @pl.when((i >= 2) & (i < 2 + NEAR))
        def _():
            k = i - 2
            near_wait(near_arr, k, out_s, out_r, True)
            near_expert(k)
            near_send(near_res, near_ret, k, home_s, home_r, sp_behind)

        @pl.when((i >= 3) & (i < far + 3))
        def _():
            chain(i - 3)[1]()

        @pl.when((i >= 4) & (i < far + 4))
        def _():
            k = i - 4
            chain(k)[2]()
            summed[k] = (
                res[k, 0].astype(F32) + res2[k, 0].astype(F32) + res2[k, 1].astype(F32)
            ).astype(BF16)
            for dg in range(groups):
                remote(
                    summed.at[k, dg // half, dg % half], ret.at[k, dg // half, dg % half],
                    back_s.at[k], back_r.at[k], sp_behind(zone(k), dg), x,
                ).start()

        @pl.when(i == NEAR + 3)
        def _():
            near_ret[NEAR - 1, 0:msg] = near_res[NEAR - 1, 0:msg]
            for k in range(NEAR):
                near_wait(near_ret, k, home_s, home_r, True)
            near_combine()
            part_begin()

        @pl.when(i == NEAR + 4)
        def _():
            part_turn()

    part_finish()

    @pl.loop(0, far)
    def _(i):
        a = ret.at[i]
        remote(a, a, back_s.at[i], back_r.at[i], s, right).wait_recv()

    for n in range(d_model // nc):
        h, c = divmod(n * nc, dh)
        cols = slice(n * nc, (n + 1) * nc)
        local = slice(c, c + nc)
        block = ret[:, :, :, :, cols].reshape(far_slots, nc)
        total = jnp.dot(wcomb[0], block, preferred_element_type=F32)
        total = total + jnp.dot(wcomb[1], block, preferred_element_type=F32)
        total = total + part[0, h, :, local].astype(F32)
        total = total + part2[0, h, :, local].astype(F32) + part2[1, h, :, local].astype(F32)
        out[:, cols] = (mid[h, :, local].astype(F32) + total).astype(BF16)

    halo_copy.wait_send()
    proj_drain()
    nrm_drain()
    part_drain()

    @pl.loop(0, far)
    def _(i):
        a = outgoing.at[i]
        remote(a, a, a2a_s.at[i], a2a_r.at[i], s, right).wait_send()
        b = summed.at[i]
        remote(b, b, back_s.at[i], back_r.at[i], s, right).wait_send()
        spread(i)[3]()
        chain(i)[3]()

    for k in range(NEAR):
        near_wait(near_out, k, out_s, out_r, False)
        near_wait(near_res, k, home_s, home_r, False)


def STEPS(far):
    return max(far + 4, NEAR + 5)


def local(
    resid, conv_b, conv_c, conv_x, conv_taps, out_weight, norm_gain, routes, route_weight,
    expert_gate, expert_up, expert_down, shared_gate, shared_up, shared_down,
):
    sp_count = lax.axis_size("sp")
    groups = max(2, sp_count // 8)
    zs = sp_count // groups
    half = groups // 2
    far = zs - NEAR
    near_slots = NEAR * groups * TP * CAP
    q, d = resid.shape
    toks, ch = conv_b.shape
    ff = expert_gate.shape[2]
    dh = d // 2
    vmem = pltpu.VMEM
    dma = pltpu.SemaphoreType.DMA
    anywhere = pl.BlockSpec(memory_space=pl.ANY)
    inside = pl.BlockSpec(memory_space=pltpu.VMEM)
    return pl.pallas_call(
        functools.partial(kernel, groups),
        out_shape=jax.ShapeDtypeStruct((q, d), BF16),
        in_specs=[anywhere] * 4 + [inside, anywhere] + [inside] * 3 + [anywhere] * 6,
        out_specs=inside,
        scratch_shapes=[
            vmem((q, d), BF16), vmem((toks, ch), BF16), vmem((toks, ch), BF16),
            vmem((toks, ch), BF16), vmem((ch, d), BF16),
            vmem((d, ff), BF16), vmem((d, ff), BF16), vmem((ff, d), BF16),
            vmem((d, ff), BF16), vmem((d, ff), BF16), vmem((ff, d), BF16),
            vmem((toks + 8, ch), F32), vmem((toks, ch), BF16), vmem((8, ch), F32), vmem((8, ch), F32),
            vmem((2, q, dh), F32),
            vmem((4, 2, q, dh), BF16), vmem((2, q, dh), BF16), vmem((2, 2, q, dh), BF16),
            vmem((2, q, dh), BF16), vmem((4, 2, q, dh), BF16),
            vmem((4, 2, q, dh), BF16), vmem((2, q, dh), BF16), vmem((2, 2, q, dh), BF16),
            vmem((4, 2, q, dh), F32),
            vmem((8, toks), F32), vmem((toks, 8), F32),
            vmem((far * groups * CAP, q), BF16), vmem((2, q, far * groups * CAP), BF16),
            vmem((far, 2, half, CAP, d), BF16),
            vmem((far, 4, 2, half, CAP, d), BF16),
            vmem((far, 4, 2, half, CAP, d), BF16),
            vmem((far, 2, half, CAP, d), BF16),
            vmem((far, 2, 2, half, CAP, d), BF16),
            vmem((far, 2, half, CAP, d), BF16),
            vmem((far, 2, half, CAP, d), BF16),
            vmem((TP, near_slots, q), BF16), vmem((2, TP, q, near_slots), BF16),
            vmem((NEAR, groups * TP * CAP, d), BF16), vmem((NEAR, groups * TP * CAP, d), BF16),
            vmem((NEAR, groups * TP * CAP, d), BF16), vmem((NEAR, groups * TP * CAP, d), BF16),
            dma((11,)), dma((2,)), dma(()), dma((6,)), dma(()), dma((4,)), dma(()), dma((6,)),
            dma((far,)), dma((far,)), dma((far,)), dma((far, 4)), dma((far,)), dma((far, 6)),
            dma((far,)), dma((far,)), dma((NEAR,)), dma((NEAR,)), dma((NEAR,)), dma((NEAR,)),
        ],
        compiler_params=pltpu.CompilerParams(
            collective_id=0, has_side_effects=True, vmem_limit_bytes=60 * 1024 * 1024
        ),
        name="layer",
    )(
        resid, conv_b, conv_c, conv_x, conv_taps, out_weight, norm_gain.reshape(1, d), routes.T,
        route_weight.T, expert_gate, expert_up, expert_down, shared_gate, shared_up, shared_down,
    )


def solution(mesh):
    return jax.shard_map(
        local,
        mesh=mesh,
        in_specs=(
            P(("sp", "tp"), None),
            P("sp", "tp"),
            P("sp", "tp"),
            P("sp", "tp"),
            P(None, "tp"),
            P("tp", None),
            P(),
            P("sp", None),
            P("sp", None),
            P("sp", None, "tp"),
            P("sp", None, "tp"),
            P("sp", "tp", None),
            P(None, "tp"),
            P(None, "tp"),
            P("tp", None),
        ),
        out_specs=P(("sp", "tp"), None),
        check_vma=False,
    )
```

time: 139 us -> 118 us (0.85)
  Pallas kernels: 135 us -> 116 us
  local copies, waits for them, and re-layouts: 4.12 us -> 1.77 us
    pallas_call x1, Pallas kernels: 135 us -> 116 us  [local(): pl.pallas_call(functools.partial(kernel, groups), out_shape=jax.ShapeDtyp...]
    unnamed x5 -> x1, local copies, waits for them, and re-layouts: 4.12 us -> 1.77 us
where the time goes in v2:
time: 118 us; the launch traced here: 117 us
  Pallas kernels  116 us (98%)
  local copies, waits for them, and re-layouts  1.77 us (2%)
    pallas_call x1, Pallas kernels, local(): pl.pallas_call(functools.partial(kernel, groups), out_shape=jax.ShapeDtyp...  116 us

profile of v2, /device:TPU:1, one launch (start us, length us, event | category | flops | bytes accessed | tf_op | source)
XLA Modules:
  0.0 117.4 jit_solution(16574960633891825905)
XLA Ops:
  0.0 115.6 %layer.1 = bf16[96,2048]{1,0:T(8,128)(2,1)} custom-call(bf16[96,2048]{1,0:T(8,128)(2,1)} %resid_h.1, bf16[384,256]{1,0:T(8,128)(2,1)} %cb_h.1, bf16[384,256]{1,0:T(8,128)(2,1)} %cc_h.1, bf16[384,256]{1,0:T(8,128)(2,1)} %cx_h.1, bf16[3,256]{1,0:T(4,128)(2,1)} %taps.1, bf16[256,2048]{1,0:T(8,128)(2,1)} %ow_h.1, f32[1,2048]{1,0:T(1,128)} %bitcast.3, ...), custom_call_target="tpu_custom_call" | custom-call | tf_op jit(solution)/shard_map/layer/pallas_call | solution.py:482
  115.7 1.8 %copy.17 = bf16[96,2048]{1,0:T(8,128)(2,1)} copy(bf16[96,2048]{1,0:T(8,128)(2,1)} %layer.1) | data formatting | bytes 786432

commit v3 on v2

--- a/solution.py
+++ b/solution.py
@@ -12,6 +12,7 @@
 CAP = 4
 TP = 4
 NEAR = 3
+NEAR_STEP = 4
 
 
 def remote(src, dst, send_sem, recv_sem, sp, tp):
@@ -40,7 +41,7 @@
     rowform, colform, disp, wcomb, outgoing, arr, res, res1, res2, summed, ret,
     near_disp, near_w, near_out, near_arr, near_res, near_ret,
     load_sem, halo_sem, proj_s, proj_r, nrm_s, nrm_r, part_s, part_r,
-    a2a_s, a2a_r, ag_s, ag_r, rs_s, rs_r, back_s, back_r, out_s, out_r, home_s, home_r,
+    a2a_s, a2a_r, ag_s, ag_r, rs_s, rs_r, back_s, back_r, out_s, out_r, home_s, home_r, known,
 ):
     s = lax.axis_index("sp")
     x = lax.axis_index("tp")
@@ -63,9 +64,13 @@
     def sp_behind(dz, dg):
         return lax.rem(z + zs - dz, zs) * groups + lax.rem(g + groups - dg, groups)
 
+    order = sorted(range(2, zs - 1), key=lambda dz: (min(dz, zs - dz) == 2, min(dz, zs - dz)))
+
     def zone(i):
-        k = lax.div(i + 1, 2)
-        return lax.rem(zs // 2 + zs + (1 - 2 * lax.rem(i, 2)) * k, zs)
+        dz = order[0]
+        for n, other in enumerate(order[1:]):
+            dz = jnp.where(i == n + 1, other, dz)
+        return dz
 
     def near_zone(k):
         return jnp.where(k == 0, 1, jnp.where(k == 1, zs - 1, 0))
@@ -80,17 +85,30 @@
 
     barrier = pltpu.get_barrier_semaphore()
 
+    def tell(sem, sp, tp):
+        pl.semaphore_signal(
+            sem, inc=1, device_id=(sp, tp), device_id_type=pl.DeviceIdType.MESH
+        )
+
+    core = z * groups + g + 1 - 2 * lax.rem(g, 2)
+    y_sides = (sp_ahead(0, 2), sp_behind(0, 2)) if groups > 2 else ()
+    z_sides = (sp_ahead(1, 0), sp_behind(1, 0))
+    ring_sides = (lax.rem(s + 1, sp_count), lax.rem(s + sp_count - 1, sp_count))
     for side in (right, left):
-        pl.semaphore_signal(
-            barrier, inc=1, device_id=(s, side), device_id_type=pl.DeviceIdType.MESH
-        )
-
-    @pl.loop(1, sp_count)
-    def _(d):
-        pl.semaphore_signal(
-            barrier, inc=1, device_id=(lax.rem(s + d, sp_count), x),
-            device_id_type=pl.DeviceIdType.MESH,
-        )
+        tell(barrier, s, side)
+    for side in ring_sides + (core,) + y_sides + z_sides:
+        tell(barrier, side, x)
+    n_near = 2 + 3 + len(y_sides) + 2
+    rounds = [(core,)] + [y_sides] * (groups // 4) + [z_sides] * (zs // 2)
+
+    def pass_on(k):
+        if k < len(rounds):
+            for side in rounds[k]:
+                tell(known.at[k], side, x)
+
+    def learn(k):
+        if k < len(rounds):
+            pl.semaphore_wait(known.at[k], len(rounds[k]))
 
     for i in range(3):
         loads[i].wait()
@@ -116,7 +134,8 @@
                 project(j), ow[:, h * dh : (h + 1) * dh], preferred_element_type=F32
             ).astype(BF16)
 
-    pl.semaphore_wait(barrier, sp_count - 1 + 2)
+    pl.semaphore_wait(barrier, n_near)
+    pass_on(0)
     halo_copy = remote(
         halo, halo_in, halo_sem.at[0], halo_sem.at[1], lax.rem(s + 1, sp_count), x
     )
@@ -171,6 +190,8 @@
     proj_begin, proj_turn, proj_finish, proj_drain = ring_sum(
         proj, proj1, proj2, proj_s, lambda k: proj_r.at[k]
     )
+    learn(0)
+    pass_on(1)
     halo_copy.wait_recv()
     prod[0:8] = halo_in[...] * jnp.where(s == 0, 0.0, 1.0)
     mix(16)
@@ -179,8 +200,13 @@
             mixed[0:16], ow[:, h * dh : (h + 1) * dh], preferred_element_type=F32
         ).astype(BF16)
     proj_begin()
+    learn(1)
+    pass_on(2)
     for h in range(2):
         own[h] = jnp.dot(project(0), ow[:, h * dh : (h + 1) * dh], preferred_element_type=F32)
+
+    learn(2)
+    pass_on(3)
 
     rowform[0:2] = routes[...].astype(F32)
     rowform[2:4] = rweight[...]
@@ -205,21 +231,26 @@
     far_slots = far * groups * CAP
     i_slot = lax.broadcasted_iota(jnp.int32, (q, far_slots), 1)
     offset = lax.div(i_slot, CAP)
-    disp[...], wcomb[0], wcomb[1] = table(
+    disp[...], wcomb[0:q], wcomb[q : 2 * q] = table(
         0, zone(lax.div(offset, groups)), lax.rem(offset, groups), lax.rem(i_slot, CAP),
         i_slot >= 0,
     )
 
+    learn(3)
+    pass_on(4)
     proj_turn()
 
     near_slots = NEAR * groups * msg
     n_slot = lax.broadcasted_iota(jnp.int32, (q, near_slots), 1)
     near_offset = lax.div(n_slot, msg)
     for j in range(TP):
-        near_disp[j], near_w[0, j], near_w[1, j] = table(
+        high, low = pl.ds(j * q, q), pl.ds((TP + j) * q, q)
+        near_disp[j], near_w[high], near_w[low] = table(
             j, near_zone(lax.div(near_offset, groups)), lax.rem(near_offset, groups),
             lax.rem(n_slot, CAP), lax.rem(lax.div(n_slot, CAP), TP) == j,
         )
+        learn(4 + j)
+        pass_on(5 + j)
 
     loads[4].wait()
     proj_finish()
@@ -239,24 +270,27 @@
 
     zone_rows = groups * CAP
 
-    @pl.loop(0, far)
-    def _(i):
-        rows = disp[pl.ds(pl.multiple_of(i * zone_rows, zone_rows), zone_rows)]
-        for h in range(2):
-            picked = jnp.dot(rows, nrm[0, h], preferred_element_type=F32)
-            outgoing[i, :, :, :, h * dh : (h + 1) * dh] = picked.astype(BF16).reshape(
-                2, half, CAP, dh
-            )
-        for dg in range(groups):
-            remote(
-                outgoing.at[i, dg // half, dg % half], arr.at[i, 0, dg // half, dg % half],
-                a2a_s.at[i], a2a_r.at[i], sp_ahead(zone(i), dg), x,
-            ).start()
-
+    def far_dispatch(low, high):
+        @pl.loop(low, high)
+        def _(i):
+            rows = disp[pl.ds(pl.multiple_of(i * zone_rows, zone_rows), zone_rows)]
+            for h in range(2):
+                picked = jnp.dot(rows, nrm[0, h], preferred_element_type=F32)
+                outgoing[i, :, :, :, h * dh : (h + 1) * dh] = picked.astype(BF16).reshape(
+                    2, half, CAP, dh
+                )
+            for dg in range(groups):
+                remote(
+                    outgoing.at[i, dg // half, dg % half], arr.at[i, 0, dg // half, dg % half],
+                    a2a_s.at[i], a2a_r.at[i], sp_ahead(zone(i), dg), x,
+                ).start()
+
+    urgent = min(3, far)
+    far_dispatch(0, urgent)
     for one in loads[5:]:
         one.wait()
     nrm_turn()
-    nrm_finish()
+    far_dispatch(urgent, far)
 
     near_rows = groups * msg
 
@@ -286,19 +320,20 @@
         def _():
             fire(ref.at[k, msg:near_rows])
 
-    @pl.loop(0, NEAR)
-    def _(k):
-        rows = pl.ds(pl.multiple_of(k * near_rows, near_rows), near_rows)
-        for h in range(2):
-            picked = jnp.dot(near_disp[0, rows], nrm[0, h], preferred_element_type=F32)
-            for j in range(1, TP):
-                picked = picked + jnp.dot(
-                    near_disp[j, rows], nrm[j, h], preferred_element_type=F32
-                )
-            near_out[k, :, h * dh : (h + 1) * dh] = picked.astype(BF16)
-        near_send(near_out, near_arr, k, out_s, out_r, sp_ahead)
-
-    near_arr[NEAR - 1, 0:msg] = near_out[NEAR - 1, 0:msg]
+    def near_dispatch():
+        @pl.loop(0, NEAR)
+        def _(k):
+            rows = pl.ds(pl.multiple_of(k * near_rows, near_rows), near_rows)
+            for h in range(2):
+                picked = jnp.dot(near_disp[0, rows], nrm[0, h], preferred_element_type=F32)
+                for j in range(1, TP):
+                    picked = picked + jnp.dot(
+                        near_disp[j, rows], nrm[j, h], preferred_element_type=F32
+                    )
+                near_out[k, :, h * dh : (h + 1) * dh] = picked.astype(BF16)
+            near_send(near_out, near_arr, k, out_s, out_r, sp_ahead)
+
+        near_arr[NEAR - 1, 0:msg] = near_out[NEAR - 1, 0:msg]
 
     def chain(i):
         return ring_sum(res.at[i], res1.at[i], res2.at[i], rs_s.at[i], lambda k: rs_r.at[i, k])
@@ -353,16 +388,26 @@
             ).reshape(TP, q, dh)
 
     def near_combine():
-        for j in range(TP):
-            for n in range(d_model // nc):
-                h, c = divmod(n * nc, dh)
-                block = near_ret[:, :, n * nc : (n + 1) * nc].reshape(near_slots, nc)
-                total = partf[j, h, :, c : c + nc]
-                total = total + jnp.dot(near_w[0, j], block, preferred_element_type=F32)
-                total = total + jnp.dot(near_w[1, j], block, preferred_element_type=F32)
-                part[j, h, :, c : c + nc] = total.astype(BF16)
-
-    @pl.loop(0, STEPS(far))
+        for n in range(d_model // kc):
+            h, c = divmod(n * kc, dh)
+            block = near_ret[:, :, n * kc : (n + 1) * kc].reshape(near_slots, kc)
+            both = jnp.dot(near_w[...], block, preferred_element_type=F32)
+            total = partf[:, h, :, c : c + kc] + (both[: TP * q] + both[TP * q :]).reshape(
+                TP, q, kc
+            )
+            part[:, h, :, c : c + kc] = total.astype(BF16)
+
+    def far_combine():
+        for n in range(d_model // nc):
+            h, c = divmod(n * nc, dh)
+            block = ret[:, :, :, :, n * nc : (n + 1) * nc].reshape(far_slots, nc)
+            both = jnp.dot(wcomb[...], block, preferred_element_type=F32)
+            own[h, :, c : c + nc] = (
+                both[:q] + both[q:] + mid[h, :, c : c + nc].astype(F32)
+                + part[0, h, :, c : c + nc].astype(F32)
+            )
+
+    @pl.loop(0, far + 4)
     def _(i):
         @pl.when(i < far)
         def _():
@@ -370,6 +415,11 @@
             remote(a, a, a2a_s.at[i], a2a_r.at[i], s, right).wait_recv()
             spread(i)[0]()
 
+        @pl.when(i == 0)
+        def _():
+            nrm_finish()
+            near_dispatch()
+
         @pl.when((i >= 1) & (i < far + 1))
         def _():
             spread(i - 1)[1]()
@@ -384,12 +434,13 @@
             far_expert(i - 2)
             chain(i - 2)[0]()
 
-        @pl.when((i >= 2) & (i < 2 + NEAR))
-        def _():
-            k = i - 2
-            near_wait(near_arr, k, out_s, out_r, True)
-            near_expert(k)
-            near_send(near_res, near_ret, k, home_s, home_r, sp_behind)
+        @pl.when(i == NEAR_STEP)
+        def _():
+            @pl.loop(0, NEAR)
+            def _(k):
+                near_wait(near_arr, k, out_s, out_r, True)
+                near_expert(k)
+                near_send(near_res, near_ret, k, home_s, home_r, sp_behind)
 
         @pl.when((i >= 3) & (i < far + 3))
         def _():
@@ -408,35 +459,23 @@
                     back_s.at[k], back_r.at[k], sp_behind(zone(k), dg), x,
                 ).start()
 
-        @pl.when(i == NEAR + 3)
-        def _():
-            near_ret[NEAR - 1, 0:msg] = near_res[NEAR - 1, 0:msg]
-            for k in range(NEAR):
-                near_wait(near_ret, k, home_s, home_r, True)
-            near_combine()
-            part_begin()
-
-        @pl.when(i == NEAR + 4)
-        def _():
-            part_turn()
-
-    part_finish()
+    near_ret[NEAR - 1, 0:msg] = near_res[NEAR - 1, 0:msg]
+    for k in range(NEAR):
+        near_wait(near_ret, k, home_s, home_r, True)
+    near_combine()
+    part_begin()
+    part_turn()
 
     @pl.loop(0, far)
     def _(i):
         a = ret.at[i]
         remote(a, a, back_s.at[i], back_r.at[i], s, right).wait_recv()
 
-    for n in range(d_model // nc):
-        h, c = divmod(n * nc, dh)
-        cols = slice(n * nc, (n + 1) * nc)
-        local = slice(c, c + nc)
-        block = ret[:, :, :, :, cols].reshape(far_slots, nc)
-        total = jnp.dot(wcomb[0], block, preferred_element_type=F32)
-        total = total + jnp.dot(wcomb[1], block, preferred_element_type=F32)
-        total = total + part[0, h, :, local].astype(F32)
-        total = total + part2[0, h, :, local].astype(F32) + part2[1, h, :, local].astype(F32)
-        out[:, cols] = (mid[h, :, local].astype(F32) + total).astype(BF16)
+    far_combine()
+    part_finish()
+    for h in range(2):
+        total = own[h] + part2[0, h].astype(F32) + part2[1, h].astype(F32)
+        out[:, h * dh : (h + 1) * dh] = total.astype(BF16)
 
     halo_copy.wait_send()
     proj_drain()
@@ -455,10 +494,6 @@
     for k in range(NEAR):
         near_wait(near_out, k, out_s, out_r, False)
         near_wait(near_res, k, home_s, home_r, False)
-
-
-def STEPS(far):
-    return max(far + 4, NEAR + 5)
 
 
 def local(
@@ -496,7 +531,7 @@
             vmem((4, 2, q, dh), BF16), vmem((2, q, dh), BF16), vmem((2, 2, q, dh), BF16),
             vmem((4, 2, q, dh), F32),
             vmem((8, toks), F32), vmem((toks, 8), F32),
-            vmem((far * groups * CAP, q), BF16), vmem((2, q, far * groups * CAP), BF16),
+            vmem((far * groups * CAP, q), BF16), vmem((2 * q, far * groups * CAP), BF16),
             vmem((far, 2, half, CAP, d), BF16),
             vmem((far, 4, 2, half, CAP, d), BF16),
             vmem((far, 4, 2, half, CAP, d), BF16),
@@ -504,12 +539,13 @@
             vmem((far, 2, 2, half, CAP, d), BF16),
             vmem((far, 2, half, CAP, d), BF16),
             vmem((far, 2, half, CAP, d), BF16),
-            vmem((TP, near_slots, q), BF16), vmem((2, TP, q, near_slots), BF16),
+            vmem((TP, near_slots, q), BF16), vmem((2 * TP * q, near_slots), BF16),
             vmem((NEAR, groups * TP * CAP, d), BF16), vmem((NEAR, groups * TP * CAP, d), BF16),
             vmem((NEAR, groups * TP * CAP, d), BF16), vmem((NEAR, groups * TP * CAP, d), BF16),
             dma((11,)), dma((2,)), dma(()), dma((6,)), dma(()), dma((4,)), dma(()), dma((6,)),
             dma((far,)), dma((far,)), dma((far,)), dma((far, 4)), dma((far,)), dma((far, 6)),
             dma((far,)), dma((far,)), dma((NEAR,)), dma((NEAR,)), dma((NEAR,)), dma((NEAR,)),
+            pltpu.SemaphoreType.REGULAR((8,)),
         ],
         compiler_params=pltpu.CompilerParams(
             collective_id=0, has_side_effects=True, vmem_limit_bytes=60 * 1024 * 1024

time: 118 us -> 109 us (0.924)
  Pallas kernels: 116 us -> 107 us
    pallas_call x1, Pallas kernels: 116 us -> 107 us  [local(): pl.pallas_call(functools.partial(kernel, groups), out_shape=jax.ShapeDtyp...]
where the time goes in v3:
time: 109 us
  Pallas kernels  107 us (98%)
  local copies, waits for them, and re-layouts  1.77 us (2%)
    pallas_call x1, Pallas kernels, local(): pl.pallas_call(functools.partial(kernel, groups), out_shape=jax.ShapeDtyp...  107 us

profile of v3, /device:TPU:1, one launch (start us, length us, event | category | flops | bytes accessed | tf_op | source)
XLA Modules:
  0.0 108.8 jit_solution(684857964315178697)
XLA Ops:
  0.0 107.1 %layer.1 = bf16[96,2048]{1,0:T(8,128)(2,1)} custom-call(bf16[96,2048]{1,0:T(8,128)(2,1)} %resid_h.1, bf16[384,256]{1,0:T(8,128)(2,1)} %cb_h.1, bf16[384,256]{1,0:T(8,128)(2,1)} %cc_h.1, bf16[384,256]{1,0:T(8,128)(2,1)} %cx_h.1, bf16[3,256]{1,0:T(4,128)(2,1)} %taps.1, bf16[256,2048]{1,0:T(8,128)(2,1)} %ow_h.1, f32[1,2048]{1,0:T(1,128)} %bitcast.3, ...), custom_call_target="tpu_custom_call" | custom-call | tf_op jit(solution)/shard_map/layer/pallas_call | solution.py:517
  107.1 1.8 %copy.17 = bf16[96,2048]{1,0:T(8,128)(2,1)} copy(bf16[96,2048]{1,0:T(8,128)(2,1)} %layer.1) | data formatting | bytes 786432

commit v4 on v3

--- a/solution.py
+++ b/solution.py
@@ -36,7 +36,7 @@
     wg_h, wu_h, wd_h, sg_h, su_h, sd_h,
     out,
     resid, cb, cc, cx, ow, wg, wu, wd, sg, su, sd,
-    prod, mixed, halo, halo_in, own, proj, proj1, proj2, mid, nrm,
+    prod, mixed, halo, halo_in, own, proj, proj1, proj2, raw, nrm,
     part, part1, part2, partf,
     rowform, colform, disp, wcomb, outgoing, arr, res, res1, res2, summed, ret,
     near_disp, near_w, near_out, near_arr, near_res, near_ret,
@@ -51,6 +51,7 @@
     half = groups // 2
     q, d_model = resid.shape
     dh = d_model // 2
+    dq = d_model // 4
     toks = cc.shape[0]
     msg = TP * CAP
     right = lax.rem(x + 1, TP)
@@ -128,10 +129,10 @@
 
     mix(toks)
     loads[3].wait()
-    for j in (2, 3, 1):
-        for h in range(2):
-            proj[j, h] = jnp.dot(
-                project(j), ow[:, h * dh : (h + 1) * dh], preferred_element_type=F32
+    for n in range(4):
+        for j in (2, 3, 1):
+            proj[n // 2, j, n % 2] = jnp.dot(
+                project(j), ow[:, n * dq : (n + 1) * dq], preferred_element_type=F32
             ).astype(BF16)
 
     pl.semaphore_wait(barrier, n_near)
@@ -142,11 +143,20 @@
     halo_copy.start()
 
     def ring_sum(b, b1, b2, ssem, rsem):
-        def begin():
+        def far_side():
             remote(b.at[2, 0], b1.at[0], ssem, rsem(0), s, right).start()
             remote(b.at[2, 1], b1.at[1], ssem, rsem(1), s, left).start()
+
+        def to_right():
             remote(b.at[3, 1], b2.at[0, 1], ssem, rsem(2), s, right).start()
+
+        def to_left():
             remote(b.at[1, 0], b2.at[1, 0], ssem, rsem(3), s, left).start()
+
+        def begin():
+            far_side()
+            to_right()
+            to_left()
 
         def turn():
             remote(b.at[2, 0], b1.at[0], ssem, rsem(0), s, left).wait_recv()
@@ -165,7 +175,7 @@
         def drain():
             remote(b.at[0:3], b.at[0:3], ssem, rsem(0), s, right).wait_send()
 
-        return begin, turn, finish, drain
+        return begin, turn, finish, drain, (far_side, to_right, to_left)
 
     def ring_gather(b, ssem, rsem):
         def begin():
@@ -187,24 +197,40 @@
 
         return begin, turn, finish, drain
 
-    proj_begin, proj_turn, proj_finish, proj_drain = ring_sum(
-        proj, proj1, proj2, proj_s, lambda k: proj_r.at[k]
-    )
+    sums = [
+        ring_sum(
+            proj.at[c], proj1.at[c], proj2.at[c], proj_s.at[c], lambda k, c=c: proj_r.at[c, k]
+        )
+        for c in range(2)
+    ]
+    gathers = [
+        ring_gather(raw.at[c], nrm_s.at[c], lambda k, c=c: nrm_r.at[c, k]) for c in range(2)
+    ]
+
+    for c in range(2):
+        pl.when(x != 2)(sums[c][4][0])
+        pl.when(x < 2)(sums[c][4][1])
+        pl.when((x == 0) | (x == 3))(sums[c][4][2])
+
     learn(0)
     pass_on(1)
     halo_copy.wait_recv()
     prod[0:8] = halo_in[...] * jnp.where(s == 0, 0.0, 1.0)
     mix(16)
-    for h in range(2):
-        proj[x, h, 0:16] = jnp.dot(
-            mixed[0:16], ow[:, h * dh : (h + 1) * dh], preferred_element_type=F32
+    for n in range(4):
+        proj[n // 2, x, n % 2, 0:16] = jnp.dot(
+            mixed[0:16], ow[:, n * dq : (n + 1) * dq], preferred_element_type=F32
         ).astype(BF16)
-    proj_begin()
+    for c in range(2):
+        pl.when(x == 2)(sums[c][4][0])
+        pl.when(x >= 2)(sums[c][4][1])
+        pl.when((x == 1) | (x == 2))(sums[c][4][2])
     learn(1)
     pass_on(2)
-    for h in range(2):
-        own[h] = jnp.dot(project(0), ow[:, h * dh : (h + 1) * dh], preferred_element_type=F32)
-
+    for n in range(4):
+        own[n // 2, n % 2] = jnp.dot(
+            project(0), ow[:, n * dq : (n + 1) * dq], preferred_element_type=F32
+        )
     learn(2)
     pass_on(3)
 
@@ -238,35 +264,51 @@
 
     learn(3)
     pass_on(4)
-    proj_turn()
+    sums[0][1]()
+    sums[1][1]()
+
+    def settle(c):
+        sums[c][2]()
+        for h in range(2):
+            n = 2 * c + h
+            total = own[c, h] + proj2[c, 0, h].astype(F32) + proj2[c, 1, h].astype(F32)
+            total = total + resid[:, n * dq : (n + 1) * dq].astype(F32)
+            raw[c, 0, h] = total.astype(BF16)
+        gathers[c][0]()
+
+    def normalize(j):
+        square = jnp.zeros((q, 1), F32)
+        for n in range(4):
+            m = raw[n // 2, j, n % 2].astype(F32)
+            square = square + jnp.sum(m * m, axis=-1, keepdims=True)
+        scale = lax.rsqrt(square * (1.0 / d_model) + 1e-06)
+        for n in range(4):
+            m = raw[n // 2, j, n % 2].astype(F32)
+            nrm[n, j] = (m * scale * gain[:, n * dq : (n + 1) * dq]).astype(BF16)
 
     near_slots = NEAR * groups * msg
     n_slot = lax.broadcasted_iota(jnp.int32, (q, near_slots), 1)
     near_offset = lax.div(n_slot, msg)
+    b_slot = lax.broadcasted_iota(jnp.int32, (q, NEAR * groups * CAP), 1)
+    b_offset = lax.div(b_slot, CAP)
     for j in range(TP):
         high, low = pl.ds(j * q, q), pl.ds((TP + j) * q, q)
-        near_disp[j], near_w[high], near_w[low] = table(
+        _, near_w[high], near_w[low] = table(
             j, near_zone(lax.div(near_offset, groups)), lax.rem(near_offset, groups),
             lax.rem(n_slot, CAP), lax.rem(lax.div(n_slot, CAP), TP) == j,
         )
+        near_disp[j], _, _ = table(
+            j, near_zone(lax.div(b_offset, groups)), lax.rem(b_offset, groups),
+            lax.rem(b_slot, CAP), b_slot >= 0,
+        )
         learn(4 + j)
         pass_on(5 + j)
-
-    loads[4].wait()
-    proj_finish()
-    square = jnp.zeros((q, 1), F32)
-    for h in range(2):
-        total = own[h] + proj2[0, h].astype(F32) + proj2[1, h].astype(F32)
-        m = (resid[:, h * dh : (h + 1) * dh].astype(F32) + total).astype(BF16)
-        mid[h] = m
-        m = m.astype(F32)
-        square = square + jnp.sum(m * m, axis=-1, keepdims=True)
-    scale = lax.rsqrt(square * (1.0 / d_model) + 1e-06)
-    for h in range(2):
-        nrm[0, h] = (mid[h].astype(F32) * scale * gain[:, h * dh : (h + 1) * dh]).astype(BF16)
-
-    nrm_begin, nrm_turn, nrm_finish, nrm_drain = ring_gather(nrm, nrm_s, lambda k: nrm_r.at[k])
-    nrm_begin()
+        if j == 1:
+            loads[4].wait()
+            settle(0)
+
+    settle(1)
+    normalize(0)
 
     zone_rows = groups * CAP
 
@@ -274,10 +316,10 @@
         @pl.loop(low, high)
         def _(i):
             rows = disp[pl.ds(pl.multiple_of(i * zone_rows, zone_rows), zone_rows)]
-            for h in range(2):
-                picked = jnp.dot(rows, nrm[0, h], preferred_element_type=F32)
-                outgoing[i, :, :, :, h * dh : (h + 1) * dh] = picked.astype(BF16).reshape(
-                    2, half, CAP, dh
+            for n in range(4):
+                picked = jnp.dot(rows, nrm[n, 0], preferred_element_type=F32)
+                outgoing[i, :, :, :, n * dq : (n + 1) * dq] = picked.astype(BF16).reshape(
+                    2, half, CAP, dq
                 )
             for dg in range(groups):
                 remote(
@@ -285,14 +327,37 @@
                     a2a_s.at[i], a2a_r.at[i], sp_ahead(zone(i), dg), x,
                 ).start()
 
-    urgent = min(3, far)
-    far_dispatch(0, urgent)
+    near_rows = groups * msg
+
+    def near_dispatch(j):
+        for n in range(4):
+            picked = jnp.dot(near_disp[j], nrm[n, j], preferred_element_type=F32)
+            near_out[:, :, j, :, n * dq : (n + 1) * dq] = picked.astype(BF16).reshape(
+                NEAR, groups, CAP, dq
+            )
+
+        @pl.loop(0, NEAR)
+        def _(k):
+            for dg in range(groups):
+                @pl.when((k != NEAR - 1) | (dg != 0))
+                def _():
+                    remote(
+                        near_out.at[k, dg, j], near_arr.at[k, dg, j], out_s.at[k], out_r.at[k],
+                        sp_ahead(near_zone(k), dg), x,
+                    ).start()
+
+    later = min(3, far)
+    far_dispatch(0, later)
+    near_dispatch(0)
     for one in loads[5:]:
         one.wait()
-    nrm_turn()
-    far_dispatch(urgent, far)
-
-    near_rows = groups * msg
+    gathers[0][1]()
+    gathers[1][1]()
+    normalize(1)
+    normalize(3)
+    far_dispatch(later, far)
+    near_dispatch(1)
+    near_dispatch(3)
 
     def near_send(src, dst, k, ssem, rsem, target):
         for dg in range(groups):
@@ -304,7 +369,7 @@
                     target(near_zone(k), dg), x,
                 ).start()
 
-    def near_wait(ref, k, ssem, rsem, recv):
+    def near_wait(k, ssem, rsem, recv):
         def fire(a):
             one = remote(a, a, ssem.at[k], rsem.at[k], s, right)
             if recv:
@@ -314,26 +379,11 @@
 
         @pl.when(k != NEAR - 1)
         def _():
-            fire(ref.at[k])
+            fire(near_res.at[k])
 
         @pl.when(k == NEAR - 1)
         def _():
-            fire(ref.at[k, msg:near_rows])
-
-    def near_dispatch():
-        @pl.loop(0, NEAR)
-        def _(k):
-            rows = pl.ds(pl.multiple_of(k * near_rows, near_rows), near_rows)
-            for h in range(2):
-                picked = jnp.dot(near_disp[0, rows], nrm[0, h], preferred_element_type=F32)
-                for j in range(1, TP):
-                    picked = picked + jnp.dot(
-                        near_disp[j, rows], nrm[j, h], preferred_element_type=F32
-                    )
-                near_out[k, :, h * dh : (h + 1) * dh] = picked.astype(BF16)
-            near_send(near_out, near_arr, k, out_s, out_r, sp_ahead)
-
-        near_arr[NEAR - 1, 0:msg] = near_out[NEAR - 1, 0:msg]
+            fire(near_res.at[k, msg:near_rows])
 
     def chain(i):
         return ring_sum(res.at[i], res1.at[i], res2.at[i], rs_s.at[i], lambda k: rs_r.at[i, k])
@@ -343,7 +393,7 @@
 
     n_rows = TP * groups * CAP
     kc = min(256, d_model)
-    nc = min(512, dh)
+    nc = dq
 
     def expert(read, write):
         gate = jnp.zeros((n_rows, wg.shape[1]), F32)
@@ -368,19 +418,19 @@
         def write(cols, value):
             near_res[k, :, cols] = value
 
-        expert(lambda cols: near_arr[k, :, cols], write)
-
-    part_begin, part_turn, part_finish, part_drain = ring_sum(
+        expert(lambda cols: near_arr[k, :, :, :, cols].reshape(n_rows, kc), write)
+
+    part_begin, part_turn, part_finish, part_drain, _ = ring_sum(
         part, part1, part2, part_s, lambda k: part_r.at[k]
     )
 
     def shared():
         gate = jnp.zeros((TP * q, sg.shape[1]), F32)
         up = jnp.zeros((TP * q, sg.shape[1]), F32)
-        for h in range(2):
-            block = nrm[:, h].reshape(TP * q, dh)
-            gate = gate + jnp.dot(block, sg[h * dh : (h + 1) * dh], preferred_element_type=F32)
-            up = up + jnp.dot(block, su[h * dh : (h + 1) * dh], preferred_element_type=F32)
+        for n in range(4):
+            block = nrm[n].reshape(TP * q, dq)
+            gate = gate + jnp.dot(block, sg[n * dq : (n + 1) * dq], preferred_element_type=F32)
+            up = up + jnp.dot(block, su[n * dq : (n + 1) * dq], preferred_element_type=F32)
         hidden = (jax.nn.silu(gate) * up).astype(BF16)
         for h in range(2):
             partf[:, h] = jnp.dot(
@@ -402,8 +452,8 @@
             h, c = divmod(n * nc, dh)
             block = ret[:, :, :, :, n * nc : (n + 1) * nc].reshape(far_slots, nc)
             both = jnp.dot(wcomb[...], block, preferred_element_type=F32)
-            own[h, :, c : c + nc] = (
-                both[:q] + both[q:] + mid[h, :, c : c + nc].astype(F32)
+            own[n // 2, n % 2] = (
+                both[:q] + both[q:] + raw[n // 2, 0, n % 2].astype(F32)
                 + part[0, h, :, c : c + nc].astype(F32)
             )
 
@@ -415,10 +465,21 @@
             remote(a, a, a2a_s.at[i], a2a_r.at[i], s, right).wait_recv()
             spread(i)[0]()
 
+        @pl.when(i == NEAR_STEP)
+        def _():
+            @pl.loop(0, NEAR)
+            def _(k):
+                near_wait(k, out_s, out_r, True)
+                near_expert(k)
+                near_send(near_res, near_ret, k, home_s, home_r, sp_behind)
+
         @pl.when(i == 0)
         def _():
-            nrm_finish()
-            near_dispatch()
+            gathers[0][2]()
+            gathers[1][2]()
+            normalize(2)
+            near_dispatch(2)
+            near_arr[NEAR - 1, 0] = near_out[NEAR - 1, 0]
 
         @pl.when((i >= 1) & (i < far + 1))
         def _():
@@ -434,17 +495,17 @@
             far_expert(i - 2)
             chain(i - 2)[0]()
 
-        @pl.when(i == NEAR_STEP)
-        def _():
-            @pl.loop(0, NEAR)
-            def _(k):
-                near_wait(near_arr, k, out_s, out_r, True)
-                near_expert(k)
-                near_send(near_res, near_ret, k, home_s, home_r, sp_behind)
-
         @pl.when((i >= 3) & (i < far + 3))
         def _():
             chain(i - 3)[1]()
+
+        @pl.when(i == far + 3)
+        def _():
+            near_ret[NEAR - 1, 0:msg] = near_res[NEAR - 1, 0:msg]
+            for k in range(NEAR):
+                near_wait(k, home_s, home_r, True)
+            near_combine()
+            part_begin()
 
         @pl.when((i >= 4) & (i < far + 4))
         def _():
@@ -459,11 +520,6 @@
                     back_s.at[k], back_r.at[k], sp_behind(zone(k), dg), x,
                 ).start()
 
-    near_ret[NEAR - 1, 0:msg] = near_res[NEAR - 1, 0:msg]
-    for k in range(NEAR):
-        near_wait(near_ret, k, home_s, home_r, True)
-    near_combine()
-    part_begin()
     part_turn()
 
     @pl.loop(0, far)
@@ -473,13 +529,16 @@
 
     far_combine()
     part_finish()
-    for h in range(2):
-        total = own[h] + part2[0, h].astype(F32) + part2[1, h].astype(F32)
-        out[:, h * dh : (h + 1) * dh] = total.astype(BF16)
+    for n in range(4):
+        h, c = divmod(n * dq, dh)
+        total = own[n // 2, n % 2] + part2[0, h, :, c : c + dq].astype(F32)
+        total = total + part2[1, h, :, c : c + dq].astype(F32)
+        out[:, n * dq : (n + 1) * dq] = total.astype(BF16)
 
     halo_copy.wait_send()
-    proj_drain()
-    nrm_drain()
+    for c in range(2):
+        sums[c][3]()
+        gathers[c][3]()
     part_drain()
 
     @pl.loop(0, far)
@@ -492,8 +551,8 @@
         chain(i)[3]()
 
     for k in range(NEAR):
-        near_wait(near_out, k, out_s, out_r, False)
-        near_wait(near_res, k, home_s, home_r, False)
+        near_wait(k, out_s, out_r, False)
+        near_wait(k, home_s, home_r, False)
 
 
 def local(
@@ -510,6 +569,7 @@
     toks, ch = conv_b.shape
     ff = expert_gate.shape[2]
     dh = d // 2
+    dq = d // 4
     vmem = pltpu.VMEM
     dma = pltpu.SemaphoreType.DMA
     anywhere = pl.BlockSpec(memory_space=pl.ANY)
@@ -525,9 +585,10 @@
             vmem((d, ff), BF16), vmem((d, ff), BF16), vmem((ff, d), BF16),
             vmem((d, ff), BF16), vmem((d, ff), BF16), vmem((ff, d), BF16),
             vmem((toks + 8, ch), F32), vmem((toks, ch), BF16), vmem((8, ch), F32), vmem((8, ch), F32),
-            vmem((2, q, dh), F32),
-            vmem((4, 2, q, dh), BF16), vmem((2, q, dh), BF16), vmem((2, 2, q, dh), BF16),
-            vmem((2, q, dh), BF16), vmem((4, 2, q, dh), BF16),
+            vmem((2, 2, q, dq), F32),
+            vmem((2, 4, 2, q, dq), BF16), vmem((2, 2, q, dq), BF16),
+            vmem((2, 2, 2, q, dq), BF16),
+            vmem((2, 4, 2, q, dq), BF16), vmem((4, 4, q, dq), BF16),
             vmem((4, 2, q, dh), BF16), vmem((2, q, dh), BF16), vmem((2, 2, q, dh), BF16),
             vmem((4, 2, q, dh), F32),
             vmem((8, toks), F32), vmem((toks, 8), F32),
@@ -539,10 +600,10 @@
             vmem((far, 2, 2, half, CAP, d), BF16),
             vmem((far, 2, half, CAP, d), BF16),
             vmem((far, 2, half, CAP, d), BF16),
-            vmem((TP, near_slots, q), BF16), vmem((2 * TP * q, near_slots), BF16),
+            vmem((TP, NEAR * groups * CAP, q), BF16), vmem((2 * TP * q, near_slots), BF16),
+            vmem((NEAR, groups, TP, CAP, d), BF16), vmem((NEAR, groups, TP, CAP, d), BF16),
             vmem((NEAR, groups * TP * CAP, d), BF16), vmem((NEAR, groups * TP * CAP, d), BF16),
-            vmem((NEAR, groups * TP * CAP, d), BF16), vmem((NEAR, groups * TP * CAP, d), BF16),
-            dma((11,)), dma((2,)), dma(()), dma((6,)), dma(()), dma((4,)), dma(()), dma((6,)),
+            dma((11,)), dma((2,)), dma((2,)), dma((2, 6)), dma((2,)), dma((2, 4)), dma(()), dma((6,)),
             dma((far,)), dma((far,)), dma((far,)), dma((far, 4)), dma((far,)), dma((far, 6)),
             dma((far,)), dma((far,)), dma((NEAR,)), dma((NEAR,)), dma((NEAR,)), dma((NEAR,)),
             pltpu.SemaphoreType.REGULAR((8,)),

time: 109 us -> 108 us (level)
    pallas_call x1, Pallas kernels: 107 us -> 106 us  [local(): pl.pallas_call(functools.partial(kernel, groups), out_shape=jax.ShapeDtyp...]
where the time goes in v4:
time: 108 us; the launch traced here: 107 us
  Pallas kernels  106 us (98%)
  local copies, waits for them, and re-layouts  1.77 us (2%)
    pallas_call x1, Pallas kernels, local(): pl.pallas_call(functools.partial(kernel, groups), out_shape=jax.ShapeDtyp...  106 us

profile of v4, /device:TPU:1, one launch (start us, length us, event | category | flops | bytes accessed | tf_op | source)
XLA Modules:
  0.0 107.4 jit_solution(15474245776810957561)
XLA Ops:
  0.0 105.6 %layer.1 = bf16[96,2048]{1,0:T(8,128)(2,1)} custom-call(bf16[96,2048]{1,0:T(8,128)(2,1)} %resid_h.1, bf16[384,256]{1,0:T(8,128)(2,1)} %cb_h.1, bf16[384,256]{1,0:T(8,128)(2,1)} %cc_h.1, bf16[384,256]{1,0:T(8,128)(2,1)} %cx_h.1, bf16[3,256]{1,0:T(4,128)(2,1)} %taps.1, bf16[256,2048]{1,0:T(8,128)(2,1)} %ow_h.1, f32[1,2048]{1,0:T(1,128)} %bitcast.3, ...), custom_call_target="tpu_custom_call" | custom-call | tf_op jit(solution)/shard_map/layer/pallas_call | solution.py:577
  105.6 1.8 %copy.17 = bf16[96,2048]{1,0:T(8,128)(2,1)} copy(bf16[96,2048]{1,0:T(8,128)(2,1)} %layer.1) | data formatting | bytes 786432

commit v5 on v4

--- a/solution.py
+++ b/solution.py
@@ -292,7 +292,7 @@
     b_slot = lax.broadcasted_iota(jnp.int32, (q, NEAR * groups * CAP), 1)
     b_offset = lax.div(b_slot, CAP)
     for j in range(TP):
-        high, low = pl.ds(j * q, q), pl.ds((TP + j) * q, q)
+        high, low = pl.ds(2 * j * q, q), pl.ds((2 * j + 1) * q, q)
         _, near_w[high], near_w[low] = table(
             j, near_zone(lax.div(near_offset, groups)), lax.rem(near_offset, groups),
             lax.rem(n_slot, CAP), lax.rem(lax.div(n_slot, CAP), TP) == j,
@@ -420,7 +420,7 @@
 
         expert(lambda cols: near_arr[k, :, :, :, cols].reshape(n_rows, kc), write)
 
-    part_begin, part_turn, part_finish, part_drain, _ = ring_sum(
+    _, part_turn, part_finish, part_drain, (part_far, part_right, part_left) = ring_sum(
         part, part1, part2, part_s, lambda k: part_r.at[k]
     )
 
@@ -437,15 +437,14 @@
                 hidden, sd[:, h * dh : (h + 1) * dh], preferred_element_type=F32
             ).reshape(TP, q, dh)
 
-    def near_combine():
-        for n in range(d_model // kc):
-            h, c = divmod(n * kc, dh)
-            block = near_ret[:, :, n * kc : (n + 1) * kc].reshape(near_slots, kc)
-            both = jnp.dot(near_w[...], block, preferred_element_type=F32)
-            total = partf[:, h, :, c : c + kc] + (both[: TP * q] + both[TP * q :]).reshape(
-                TP, q, kc
-            )
-            part[:, h, :, c : c + kc] = total.astype(BF16)
+    def near_combine(j):
+        weights = near_w[2 * j * q : 2 * (j + 1) * q]
+        for n in range(d_model // nc):
+            h, c = divmod(n * nc, dh)
+            block = near_ret[:, :, n * nc : (n + 1) * nc].reshape(near_slots, nc)
+            both = jnp.dot(weights, block, preferred_element_type=F32)
+            total = partf[j, h, :, c : c + nc] + both[:q] + both[q:]
+            part[j, h, :, c : c + nc] = total.astype(BF16)
 
     def far_combine():
         for n in range(d_model // nc):
@@ -504,8 +503,8 @@
             near_ret[NEAR - 1, 0:msg] = near_res[NEAR - 1, 0:msg]
             for k in range(NEAR):
                 near_wait(k, home_s, home_r, True)
-            near_combine()
-            part_begin()
+            near_combine(2)
+            part_far()
 
         @pl.when((i >= 4) & (i < far + 4))
         def _():
@@ -520,6 +519,11 @@
                     back_s.at[k], back_r.at[k], sp_behind(zone(k), dg), x,
                 ).start()
 
+    near_combine(3)
+    part_right()
+    near_combine(1)
+    part_left()
+    near_combine(0)
     part_turn()
 
     @pl.loop(0, far)
@@ -576,7 +580,7 @@
     inside = pl.BlockSpec(memory_space=pltpu.VMEM)
     return pl.pallas_call(
         functools.partial(kernel, groups),
-        out_shape=jax.ShapeDtypeStruct((q, d), BF16),
+        out_shape=pltpu.VMEM((q, d), BF16),
         in_specs=[anywhere] * 4 + [inside, anywhere] + [inside] * 3 + [anywhere] * 6,
         out_specs=inside,
         scratch_shapes=[

time: 108 us -> 105 us (0.972)
  Pallas kernels: 106 us -> 104 us
    pallas_call x1, Pallas kernels: 106 us -> 104 us  [local(): pl.pallas_call(functools.partial(kernel, groups), out_shape=pltpu.VMEM((q...]
where the time goes in v5:
time: 105 us; the launch traced here: 104 us
  Pallas kernels  104 us (99%)
    pallas_call x1, Pallas kernels, local(): pl.pallas_call(functools.partial(kernel, groups), out_shape=pltpu.VMEM((q...  104 us

profile of v5, /device:TPU:1, one launch (start us, length us, event | category | flops | bytes accessed | tf_op | source)
XLA Modules:
  0.0 104.5 jit_solution(17192703566119054011)
XLA Ops:
  0.0 103.7 %layer.1 = bf16[96,2048]{1,0:T(8,128)(2,1)S(1)} custom-call(bf16[96,2048]{1,0:T(8,128)(2,1)} %resid_h.1, bf16[384,256]{1,0:T(8,128)(2,1)} %cb_h.1, bf16[384,256]{1,0:T(8,128)(2,1)} %cc_h.1, bf16[384,256]{1,0:T(8,128)(2,1)} %cx_h.1, bf16[3,256]{1,0:T(4,128)(2,1)} %taps.1, bf16[256,2048]{1,0:T(8,128)(2,1)} %ow_h.1, f32[1,2048]{1,0:T(1,128)} %bitcast.3, ...), custom_call_target="tpu_custom_call" | custom-call | tf_op jit(solution)/shard_map/layer/pallas_call | solution.py:581
  103.7 0.7 copy.17

commit v6 on v5

--- a/solution.py
+++ b/solution.py
@@ -65,7 +65,7 @@
     def sp_behind(dz, dg):
         return lax.rem(z + zs - dz, zs) * groups + lax.rem(g + groups - dg, groups)
 
-    order = sorted(range(2, zs - 1), key=lambda dz: (min(dz, zs - dz) == 2, min(dz, zs - dz)))
+    order = sorted(range(2, zs - 1), key=lambda dz: (min(dz, zs - dz) != 3, min(dz, zs - dz)))
 
     def zone(i):
         dz = order[0]
@@ -525,25 +525,10 @@
     part_left()
     near_combine(0)
     part_turn()
-
-    @pl.loop(0, far)
-    def _(i):
-        a = ret.at[i]
-        remote(a, a, back_s.at[i], back_r.at[i], s, right).wait_recv()
-
-    far_combine()
-    part_finish()
-    for n in range(4):
-        h, c = divmod(n * dq, dh)
-        total = own[n // 2, n % 2] + part2[0, h, :, c : c + dq].astype(F32)
-        total = total + part2[1, h, :, c : c + dq].astype(F32)
-        out[:, n * dq : (n + 1) * dq] = total.astype(BF16)
-
     halo_copy.wait_send()
     for c in range(2):
         sums[c][3]()
         gathers[c][3]()
-    part_drain()
 
     @pl.loop(0, far)
     def _(i):
@@ -557,6 +542,20 @@
     for k in range(NEAR):
         near_wait(k, out_s, out_r, False)
         near_wait(k, home_s, home_r, False)
+
+    @pl.loop(0, far)
+    def _(i):
+        a = ret.at[i]
+        remote(a, a, back_s.at[i], back_r.at[i], s, right).wait_recv()
+
+    far_combine()
+    part_finish()
+    for n in range(4):
+        h, c = divmod(n * dq, dh)
+        total = own[n // 2, n % 2] + part2[0, h, :, c : c + dq].astype(F32)
+        total = total + part2[1, h, :, c : c + dq].astype(F32)
+        out[:, n * dq : (n + 1) * dq] = total.astype(BF16)
+    part_drain()
 
 
 def local(

time: 105 us -> 104 us (level)
  the two profiles are of different devices: /device:TPU:1 before, /device:TPU:66 now
where the time goes in v6:
time: 104 us
  Pallas kernels  104 us (100%)
    pallas_call x1, Pallas kernels, local(): pl.pallas_call(functools.partial(kernel, groups), out_shape=pltpu.VMEM((q...  104 us

profile of v6, /device:TPU:66, one launch (start us, length us, event | category | flops | bytes accessed | tf_op | source)
XLA Modules:
  0.0 104.3 jit_solution(17735792605483070698)
XLA Ops:
  0.0 103.5 %layer.1 = bf16[96,2048]{1,0:T(8,128)(2,1)S(1)} custom-call(bf16[96,2048]{1,0:T(8,128)(2,1)} %resid_h.1, bf16[384,256]{1,0:T(8,128)(2,1)} %cb_h.1, bf16[384,256]{1,0:T(8,128)(2,1)} %cc_h.1, bf16[384,256]{1,0:T(8,128)(2,1)} %cx_h.1, bf16[3,256]{1,0:T(4,128)(2,1)} %taps.1, bf16[256,2048]{1,0:T(8,128)(2,1)} %ow_h.1, f32[1,2048]{1,0:T(1,128)} %bitcast.3, ...), custom_call_target="tpu_custom_call" | custom-call | tf_op jit(solution)/shard_map/layer/pallas_call | solution.py:580
  103.5 0.7 copy.17
